TPU v7x, 512 devices: a whole 4x4x16 slice. The times are simulated.
512 devices in a mesh: sp: 64 (over z, y), tp: 8 (over x, core).
Axes of the slice: x: 4, y: 4, z: 16, core: 2. Of those that a mesh axis runs over, the one named last changes fastest.
Arguments:
- latent: bfloat16 [49152, 2048], P(('sp', 'tp')), may hold values from -6 to 6
- condition: float32 [2048], P('sp'), may hold values from -6 to 6
- context_condition: float32 [2048], P('sp'), may hold values from -6 to 6
- context: bfloat16 [1024, 2048], P('sp'), may hold values from -6 to 6
- norm_gain: float32 [2048], replicated, may hold values from 0.1 to 1.9
- shift_weight: bfloat16 [2048, 2048], P('sp', 'tp'), may hold values from -0.375 to 0.375
- scale_weight: bfloat16 [2048, 2048], P('sp', 'tp'), may hold values from -0.375 to 0.375
- gate_weight: bfloat16 [2048, 2048], P('sp', 'tp'), may hold values from -0.375 to 0.375
- query_weight: bfloat16 [2048, 2048], P(None, 'tp'), may hold values from -2 to 2
- key_matrix: bfloat16 [2048, 1024], P(None, 'tp'), may hold values from -2 to 2
- value_matrix: bfloat16 [2048, 1024], P(None, 'tp'), may hold values from -0.125 to 0.125
- sink_logit_head: float32 [16], P('tp'), may hold values from 6 to 10
- out_weight: bfloat16 [2048, 2048], P('tp'), may hold values from -0.125 to 0.125
Outputs:
- updated: bfloat16 [49152, 2048], P(('sp', 'tp'))
All inputs are finite; a program needn't handle non-finite values.
Results may differ from a plain program's by a relative error of at most 0.012.
The roundings to bfloat16 on the way count: a program that leaves them out, or rounds other values in their place, can miss the bound.
Values may be sent and summed in bfloat16 or wider, within the bound.
A program may use at most 64 MiB of HBM per device.

v0:
```python
import functools

import jax
import jax.numpy as jnp
from jax import lax
from jax.sharding import Mesh
from jax.sharding import PartitionSpec as P

QUERY_HEADS = 16
KEY_VALUE_HEADS = 8
HEAD_DIM = 128
WINDOW_REACH = 128
GRID_W = 64
SP = ("sp_0", "sp_1")
SP_TP = ("sp_0", "sp_1", "tp")


NORM_EPS = 1e-05
MASKED_SCORE = -1e30


def one_axis_at_a_time(x, axes):
    return functools.reduce(lax.psum, axes, x)


def side_by_side(arrays, axis, dim, along):
    both = jnp.concatenate(arrays, axis=along)
    out, at, outs = (lax.all_gather(both, axis, axis=dim, tiled=True), 0, [])
    for a in arrays:
        outs.append(lax.slice_in_dim(out, at, at + a.shape[along], axis=along))
        at += a.shape[along]
    return tuple(outs)


def padded_2(block, sides, width):
    for axis, dim in sides:
        count = lax.axis_size(axis)
        forward = [(i, i + 1) for i in range(count - 1)]
        backward = [(target, source) for source, target in forward]
        low = lax.ppermute(
            lax.slice_in_dim(block, block.shape[dim] - width, None, axis=dim), axis, forward
        )
        high = lax.ppermute(lax.slice_in_dim(block, 0, width, axis=dim), axis, backward)
        block = jnp.concatenate([low, block, high], axis=dim)
    return block


def sent_to_all(x, axis):
    peers = lax.axis_size(axis)
    return lax.all_to_all(jnp.broadcast_to(x[None], (peers, *x.shape)), axis, 0, 0, tiled=True)


def laid_out(blocks, dim):
    blocks = jnp.moveaxis(blocks, 0, dim)
    shape = blocks.shape
    return blocks.reshape(*shape[:dim], shape[dim] * shape[dim + 1], *shape[dim + 2 :])


def gathered_copies(x, axis, dim):
    blocks = sent_to_all(x, axis)
    return laid_out(blocks, dim)


def in_blocks(x, dim, peers):
    before, after = (x.shape[:dim], x.shape[dim + 1 :])
    return jnp.moveaxis(x.reshape(*before, peers, -1, *after), dim, 0)


def summed_on_arrival(x, axis, dim):
    peers = lax.axis_size(axis)
    blocks = lax.all_to_all(in_blocks(x, dim, peers), axis, 0, 0, tiled=True)
    return jnp.sum(blocks.astype(jnp.float32), axis=0)


def rotate(vectors, position):
    quarter = HEAD_DIM // 4
    grid_row = (position // GRID_W).astype(jnp.float32)
    grid_col = (position % GRID_W).astype(jnp.float32)
    inv_freq = 10000.0 ** (-jnp.arange(0, HEAD_DIM // 2, 2, dtype=jnp.float32) / (HEAD_DIM // 2))
    angles = jnp.concatenate([grid_row[:, None] * inv_freq, grid_col[:, None] * inv_freq], axis=-1)
    cosine_table = jnp.cos(angles).reshape(-1, 1, 2, quarter)
    sine_table = jnp.sin(angles).reshape(-1, 1, 2, quarter)
    pieces = vectors.reshape(vectors.shape[0], vectors.shape[1], 2, 2, quarter)
    first_half = pieces[..., 0, :]
    second_half = pieces[..., 1, :]
    turned = jnp.stack(
        [
            first_half * cosine_table - second_half * sine_table,
            first_half * sine_table + second_half * cosine_table,
        ],
        axis=-2,
    )
    return turned.reshape(vectors.shape)


def modulated_norm(rows_in, norm_gain, shift, scale):
    floats = rows_in.astype(jnp.float32)
    normed = (
        floats * lax.rsqrt(jnp.mean(floats * floats, axis=-1, keepdims=True) + NORM_EPS) * norm_gain
    )
    return (normed * (1.0 + scale) + shift).astype(jnp.bfloat16)


def shards(
    latent,
    condition,
    context_condition,
    context,
    norm_gain,
    shift_weight,
    scale_weight,
    gate_weight,
    query_weight,
    key_matrix,
    value_matrix,
    sink_logit_head,
    out_weight,
):
    tp_count = lax.axis_size("tp")
    group_rows = latent.shape[0] * tp_count
    offset = lax.axis_index(SP) * group_rows
    total_rows = group_rows * lax.axis_size(SP)
    active = jax.nn.silu(jnp.stack([condition, context_condition])).astype(jnp.bfloat16)
    shift_part = jnp.dot(active, shift_weight, preferred_element_type=jnp.float32)
    scale_part = jnp.dot(active, scale_weight, preferred_element_type=jnp.float32)
    gate_part = jnp.dot(active[:1], gate_weight, preferred_element_type=jnp.float32)
    shift_sum, scale_sum, gate_sum = (
        one_axis_at_a_time(shift_part, SP),
        one_axis_at_a_time(scale_part, SP),
        one_axis_at_a_time(gate_part, SP),
    )
    shift_all, scale_all, gate_all = side_by_side((shift_sum, scale_sum, gate_sum), "tp", 1, 0)
    hidden_state = modulated_norm(latent, norm_gain, shift_all[0], scale_all[0])
    query_width = query_weight.shape[1]
    pair_width = key_matrix.shape[1]
    block_rows = lax.all_gather(hidden_state, "tp", axis=0, tiled=True)
    row_count = block_rows.shape[0]
    position = offset + jnp.arange(row_count, dtype=jnp.int32)
    query_row_block = jnp.dot(block_rows, query_weight, preferred_element_type=jnp.float32)
    query_row_block = rotate(query_row_block.reshape(row_count, -1, HEAD_DIM), position)
    key_rows = jnp.dot(block_rows, key_matrix, preferred_element_type=jnp.float32)
    key_rows = rotate(key_rows.reshape(row_count, -1, HEAD_DIM), position)
    value_rows = jnp.dot(block_rows, value_matrix, preferred_element_type=jnp.float32)
    projected = jnp.concatenate(
        [
            query_row_block.reshape(row_count, query_width),
            key_rows.reshape(row_count, pair_width),
            value_rows,
        ],
        axis=1,
    ).astype(jnp.bfloat16)
    padded = padded_2(projected[:, query_width:], ((SP, 0),), WINDOW_REACH)
    ctx_hidden = modulated_norm(context, norm_gain, shift_all[1], scale_all[1])
    ctx_pairs = gathered_copies(
        jnp.concatenate(
            [
                jnp.dot(ctx_hidden, key_matrix, preferred_element_type=jnp.float32),
                jnp.dot(ctx_hidden, value_matrix, preferred_element_type=jnp.float32),
            ],
            axis=1,
        ).astype(jnp.bfloat16),
        SP,
        0,
    )
    blocks = group_rows // WINDOW_REACH
    kv_local = pair_width // HEAD_DIM
    queries_per_group = QUERY_HEADS // KEY_VALUE_HEADS
    query_blocks = projected[:, :query_width].reshape(
        blocks, WINDOW_REACH, kv_local, queries_per_group, HEAD_DIM
    )
    key_pad = padded[:, :pair_width].reshape(blocks + 2, WINDOW_REACH, kv_local, HEAD_DIM)
    value_pad = padded[:, pair_width:].reshape(blocks + 2, WINDOW_REACH, kv_local, HEAD_DIM)
    band_keys = jnp.concatenate([key_pad[:-2], key_pad[1:-1], key_pad[2:]], axis=1)
    band_values = jnp.concatenate([value_pad[:-2], value_pad[1:-1], value_pad[2:]], axis=1)
    context_key_rows = ctx_pairs[:, :pair_width].reshape(-1, kv_local, HEAD_DIM)
    context_value_rows = ctx_pairs[:, pair_width:].reshape(-1, kv_local, HEAD_DIM)
    factor = HEAD_DIM ** (-0.5)
    band_scores = (
        jnp.einsum("nqhgd,nkhd->nhgqk", query_blocks, band_keys, preferred_element_type=jnp.float32)
        * factor
    )
    block_ids = jnp.arange(blocks, dtype=jnp.int32)[:, None, None]
    query_pos = (
        offset + block_ids * WINDOW_REACH + jnp.arange(WINDOW_REACH, dtype=jnp.int32)[None, :, None]
    )
    key_pos = (
        offset
        + (block_ids - 1) * WINDOW_REACH
        + jnp.arange(3 * WINDOW_REACH, dtype=jnp.int32)[None, None, :]
    )
    allowed = (
        (jnp.abs(key_pos - query_pos) <= WINDOW_REACH) & (key_pos >= 0) & (key_pos < total_rows)
    )
    band_scores = jnp.where(allowed[:, None, None], band_scores, MASKED_SCORE)
    ctx_scores = (
        jnp.einsum(
            "nqhgd,chd->nhgqc", query_blocks, context_key_rows, preferred_element_type=jnp.float32
        )
        * factor
    )
    sink_logit_rows = sink_logit_head.reshape(1, kv_local, queries_per_group, 1, 1)
    maxima = jnp.maximum(
        jnp.maximum(
            jnp.max(band_scores, axis=-1, keepdims=True),
            jnp.max(ctx_scores, axis=-1, keepdims=True),
        ),
        sink_logit_rows,
    )
    band_exp = jnp.exp(band_scores - maxima)
    ctx_exp = jnp.exp(ctx_scores - maxima)
    denominator = (
        jnp.sum(band_exp, axis=-1, keepdims=True)
        + jnp.sum(ctx_exp, axis=-1, keepdims=True)
        + jnp.exp(sink_logit_rows - maxima)
    )
    band_weights = (band_exp / denominator).astype(jnp.bfloat16)
    ctx_weights = (ctx_exp / denominator).astype(jnp.bfloat16)
    attended = jnp.einsum(
        "nhgqk,nkhd->nqhgd", band_weights, band_values, preferred_element_type=jnp.float32
    ) + jnp.einsum(
        "nhgqc,chd->nqhgd", ctx_weights, context_value_rows, preferred_element_type=jnp.float32
    )
    attended = attended.astype(jnp.bfloat16).reshape(group_rows, query_width)
    mixed_sum = summed_on_arrival(
        jnp.dot(attended, out_weight, preferred_element_type=jnp.float32).astype(jnp.bfloat16),
        "tp",
        0,
    )
    return (latent.astype(jnp.float32) + gate_all[0] * mixed_sum).astype(jnp.bfloat16)


def solution(mesh):
    torus = Mesh(mesh.devices.reshape(16, 4, mesh.shape["tp"]), ("sp_0", "sp_1", "tp"))
    return jax.shard_map(
        shards,
        mesh=torus,
        in_specs=(
            P(SP_TP, None),
            P(SP),
            P(SP),
            P(SP, None),
            P(),
            P(SP, "tp"),
            P(SP, "tp"),
            P(SP, "tp"),
            P(None, "tp"),
            P(None, "tp"),
            P(None, "tp"),
            P("tp"),
            P("tp", None),
        ),
        out_specs=P(SP_TP, None),
        check_vma=False,
    )
```

profile of v0, /device:TPU:1, one launch (start us, length us, event | category | flops | bytes accessed | tf_op | source)
XLA Modules:
  0.0 187.6 jit_solution(3284651303342493575)
XLA Ops:
  6.6 1.3 fusion.20
  7.9 0.7 fusion.58
  8.6 0.8 fusion.59
  9.4 0.8 fusion.71
  10.3 0.8 fusion.70
  11.1 30.7 %all-reduce = (f32[1,256]{1,0:T(1,128)S(1)}, f32[2,256]{1,0:T(2,128)S(1)}, f32[2,256]{1,0:T(2,128)S(1)}) all-reduce(f32[1,256]{1,0:T(1,128)S(1)} %fusion.59, f32[2,256]{1,0:T(2,128)S(1)} %fusion.71, f32[2,256]{1,0:T(2,128)S(1)} %fusion.70), channel_id=1, replica_groups=mesh['sp_0'=16,'sp_1'=4,'tp'=8] {'sp_0'}, use_global_device_ids=true, to_apply=%region_4.5 | all-reduce | flops 1280 | bytes 10240 | tf_op jit(solution)/shard_map/psum | solution.py:23
  41.8 8.8 %all-reduce.1 = (f32[1,256]{1,0:T(1,128)S(1)}, f32[2,256]{1,0:T(2,128)S(1)}, f32[2,256]{1,0:T(2,128)S(1)}) all-reduce(f32[1,256]{1,0:T(1,128)S(1)} %get-tuple-element.5, f32[2,256]{1,0:T(2,128)S(1)} %get-tuple-element.6, f32[2,256]{1,0:T(2,128)S(1)} %get-tuple-element.7), channel_id=1, replica_groups=mesh['sp_0'=16,'sp_1'=4,'tp'=8] {'sp_1'}, use_global_device_ids=true, to_apply=%region_5.6 | all-reduce | flops 1280 | bytes 10240 | tf_op jit(solution)/shard_map/psum | solution.py:23
  50.7 22.7 %all_gather.6 = f32[5,2048]{1,0:T(8,128)S(1)} all-gather(f32[5,256]{1,0:T(8,128)S(1)} %pad_maximum_fusion.12), channel_id=1, replica_groups=mesh['sp_0'=16,'sp_1'=4,'tp'=8] {'tp'}, dimensions={1}, use_global_device_ids=true | all-gather | bytes 46080 | tf_op jit(solution)/shard_map/all_gather | solution.py:28
  73.4 2.0 %fusion.24 = bf16[96,2048]{1,0:T(8,128)(2,1)} fusion(bf16[96,2048]{1,0:T(8,128)(2,1)} %param.13, f32[2048]{0:T(1024)S(1)} %bitcast.156, f32[2048]{0:T(1024)S(1)} %bitcast.157, f32[2048]{0:T(1024)} %param.17, f32[96]{0:T(128)S(1)} %add_rsqrt_fusion.1), kind=kLoop, calls=%fused_computation.34 | loop fusion | flops 1179648 | bytes 811392 | tf_op jit(solution)/shard_map/convert_element_type | solution.py:101
  75.4 1.0 fusion.42
  76.4 1.3 convolution_convert_fusion.2
  78.0 0.8 broadcast_in_dim.12
  78.9 7.6 %all-to-all-start = ((bf16[64,16,256]{2,1,0:T(8,128)(2,1)}), bf16[64,16,256]{2,1,0:T(8,128)(2,1)S(1)}, u32[]{:S(2)}, u32[]{:S(2)}) async-start(bf16[64,16,256]{2,1,0:T(8,128)(2,1)} %broadcast_in_dim.12), calls=%async_computation | async-start | bytes 1048576 | tf_op jit(solution)/shard_map/all_to_all | solution.py:50
  87.6 1.4 fusion.18
  89.0 14.9 %all-gather.2.cloned.1.call-done = bf16[768,2048]{1,0:T(8,128)(2,1)} async-done(((bf16[96,2048]{1,0:T(8,128)(2,1)}), bf16[768,2048]{1,0:T(8,128)(2,1)}) %all-gather.2.cloned.1.call-update) | async-done | bytes 3145744 | tf_op jit(solution)/shard_map/all_gather | solution.py:136
  103.9 3.0 %fusion.72 = f32[768,128]{0,1:T(8,128)S(1)} fusion(bf16[768,2048]{1,0:T(8,128)(2,1)} %all-gather.2.cloned.1.call-done, bf16[2048,128]{1,0:T(8,128)(2,1)S(1)} %copy-done.3), kind=kOutput, calls=%fused_computation.126 | convolution fusion | flops 402653184 | bytes 4063232 | tf_op jit(solution)/shard_map/dot_general | solution.py:141
  106.9 0.7 subtract_convert_fusion.1
  107.9 3.0 %convolution_convert_fusion.1 = bf16[768,128]{1,0:T(8,128)(2,1)S(1)} fusion(bf16[768,2048]{1,0:T(8,128)(2,1)} %all-gather.2.cloned.1.call-done, bf16[2048,128]{1,0:T(8,128)(2,1)S(1)} %copy-done.5), kind=kOutput, calls=%fused_computation.27 | convolution fusion | flops 402751488 | bytes 3866624 | tf_op jit(solution)/shard_map/dot_general | solution.py:143
  111.6 3.1 %collective-permute-start = (bf16[128,256]{1,0:T(8,128)(2,1)}, bf16[128,256]{1,0:T(8,128)(2,1)S(1)}, u32[]{:S(2)}, u32[]{:S(2)}) collective-permute-start(bf16[128,256]{1,0:T(8,128)(2,1)} %get-tuple-element.21), channel_id=1, source_target_pairs={{0,8},{8,16},{16,24},{24,32},{32,40},{40,48},{48,56},{56,64},{64,7... | collective-permute-start | bytes 196616 | tf_op jit(solution)/shard_map/ppermute | solution.py:40
  114.7 1.5 collective-permute-start.1
  116.2 1.1 fusion.73
  118.2 3.7 %bitcast_reduce_fusion = (f32[6,2,128]{2,1,0:T(2,128)S(1)}, f32[1024,6,128,2]{2,0,3,1:T(8,128)}) fusion(bf16[6,128,2,128]{3,1,2,0:T(8,128)(2,1)S(1)} %copy.27, bf16[1024,256]{1,0:T(8,128)(2,1)S(1)} %bitcast.144), kind=kOutput, calls=%fused_computation.1 | convolution fusion | flops 405797376 | bytes 6952960 | tf_op jit(solution)/shard_map/nqhgd,chd->nhgqc/dot_general | solution.py:196
  122.1 0.8 copy.24
  123.2 0.8 pad_maximum_fusion.6
  124.4 1.5 fusion.6
  126.0 3.8 %fusion.1 = f32[6,2,128]{2,1,0:T(2,128)S(1)} fusion(f32[1024,6,128,2]{2,0,3,1:T(8,128)} %get-tuple-element.41, f32[6,2,128]{2,1,0:T(2,128)S(1)} %maximum_maximum_fusion), kind=kLoop, calls=%fused_computation.5 | loop fusion | flops 4717056 | bytes 6303744 | tf_op jit(solution)/shard_map/reduce_sum | solution.py:213
  130.7 0.8 convolution_bitcast_fusion
  132.1 0.9 slice-done.1
  133.0 1.5 fusion.13
  134.9 1.0 convolution_convert_fusion
  135.9 42.9 %all_to_all.10 = bf16[8,96,2048]{2,1,0:T(8,128)(2,1)S(1)} all-to-all(bf16[8,96,2048]{2,1,0:T(8,128)(2,1)S(1)} %bitcast.139), channel_id=1, replica_groups=mesh['sp_0'=16,'sp_1'=4,'tp'=8] {'tp'}, dimensions={0} | all-to-all | bytes 6291456 | tf_op jit(solution)/shard_map/all_to_all | solution.py:71
  179.9 0.8 fusion.25
  (59 shorter events, 6.9 us)
Async XLA Ops:
  6.5 128.4 %copy-start = (bf16[256,2048]{1,0:T(8,128)(2,1)S(1)}, bf16[256,2048]{1,0:T(8,128)(2,1)}, u32[]{:S(2)}) copy-start(bf16[256,2048]{1,0:T(8,128)(2,1)} %param.25) | copy-start | bytes 3145732
  6.5 71.2 %copy-start.7 = (f32[2048]{0:T(1024)S(1)}, f32[2048]{0:T(1024)}, u32[]{:S(2)}) copy-start(f32[2048]{0:T(1024)} %param.17) | copy-start | bytes 24580
  6.5 71.2 %copy-start.4 = (bf16[16,2048]{1,0:T(8,128)(2,1)S(1)}, bf16[16,2048]{1,0:T(8,128)(2,1)}, u32[]{:S(2)}) copy-start(bf16[16,2048]{1,0:T(8,128)(2,1)} %param.16) | copy-start | bytes 196612
  6.5 71.2 %copy-start.3 = (bf16[2048,128]{1,0:T(8,128)(2,1)S(1)}, bf16[2048,128]{1,0:T(8,128)(2,1)}, u32[]{:S(2)}) copy-start(bf16[2048,128]{1,0:T(8,128)(2,1)} %param.22) | copy-start | bytes 1572868
  6.5 97.3 %all-gather.2.cloned.1.call-start = ((), (), s32[]{:S(2)}) async-start(), calls=%async_computation.2 | async-start | bytes 3538944 | tf_op jit(solution)/shard_map/all_gather | solution.py:136
  78.9 39.4 %all-to-all-start = ((bf16[64,16,256]{2,1,0:T(8,128)(2,1)}), bf16[64,16,256]{2,1,0:T(8,128)(2,1)S(1)}, u32[]{:S(2)}, u32[]{:S(2)}) async-start(bf16[64,16,256]{2,1,0:T(8,128)(2,1)} %broadcast_in_dim.12), calls=%async_computation | async-start | bytes 1048576 | tf_op jit(solution)/shard_map/all_to_all | solution.py:50
  89.0 18.9 %copy-start.5 = (bf16[2048,128]{1,0:T(8,128)(2,1)S(1)}, bf16[2048,128]{1,0:T(8,128)(2,1)}, u32[]{:S(2)}) copy-start(bf16[2048,128]{1,0:T(8,128)(2,1)} %param.23) | copy-start | bytes 1572868
  107.8 8.3 %copy-start.2 = (bf16[768,2048]{1,0:T(8,128)(2,1)S(1)}, bf16[768,2048]{1,0:T(8,128)(2,1)}, u32[]{:S(2)}) copy-start(bf16[768,2048]{1,0:T(8,128)(2,1)} %all-gather.2.cloned.1.call-done) | copy-start | bytes 9437188
  107.9 8.3 %copy-start.9 = (bf16[2048,256]{1,0:T(8,128)(2,1)S(1)}, bf16[2048,256]{1,0:T(8,128)(2,1)}, u32[]{:S(2)}) copy-start(bf16[2048,256]{1,0:T(8,128)(2,1)} %param.21) | copy-start | bytes 3145732
  111.6 11.6 %collective-permute-start = (bf16[128,256]{1,0:T(8,128)(2,1)}, bf16[128,256]{1,0:T(8,128)(2,1)S(1)}, u32[]{:S(2)}, u32[]{:S(2)}) collective-permute-start(bf16[128,256]{1,0:T(8,128)(2,1)} %get-tuple-element.21), channel_id=1, source_target_pairs={{0,8},{8,16},{16,24},{24,32},{32,40},{40,48},{48,56},{56,64},{64,7... | collective-permute-start | bytes 196616 | tf_op jit(solution)/shard_map/ppermute | solution.py:40
  114.7 8.5 %collective-permute-start.1 = (bf16[128,256]{1,0:T(8,128)(2,1)}, bf16[128,256]{1,0:T(8,128)(2,1)S(1)}, u32[]{:S(2)}, u32[]{:S(2)}) collective-permute-start(bf16[128,256]{1,0:T(8,128)(2,1)} %get-tuple-element.22), channel_id=1, source_target_pairs={{8,0},{16,8},{24,16},{32,24},{40,32},{48,40},{56,48},{64,56},{72,6... | collective-permute-start | bytes 196616 | tf_op jit(solution)/shard_map/ppermute | solution.py:43
  124.4 1.5 copy-start.8
  129.8 0.9 copy-start.6
  129.8 2.3 %slice-start = ((s8[6291456]{0:T(1024)(128)(4,1)}), s8[4194304]{0:T(1024)(128)(4,1)S(1)}, s32[]{:S(2)}) async-start(s8[6291456]{0:T(1024)(128)(4,1)} %bitcast.137), calls=%async_computation.3 | async-start | bytes 8388608
  130.7 2.2 %slice-start.1 = ((s8[6291456]{0:T(1024)(128)(4,1)}), s8[2097152]{0:T(1024)(128)(4,1)S(1)}, s32[]{:S(2)}) async-start(s8[6291456]{0:T(1024)(128)(4,1)} %bitcast.137), calls=%async_computation.4 | async-start | bytes 4194304
  178.9 1.0 copy-start.1
Sparse Core Ops, SparseCore 0:
  75.5 28.2 all-gather.1
where the time goes:
time: 189 us; the launch traced here: 188 us
  blocking collectives  105 us (56%)
  matrix products  19.8 us (10%)
  other arithmetic  15.8 us (8%)
  waiting for transfers between devices  14.9 us (8%)
  between operations  13.8 us (7%)
  starting transfers between devices  12.2 us (6%)
  local copies, waits for them, and re-layouts  5.96 us (3%)
    all_to_all x1, blocking collectives, summed_on_arrival(): blocks = lax.all_to_all(in_blocks(x, dim, peers), axis, 0, 0, tiled=True)  42.9 us
    psum x2, blocking collectives, one_axis_at_a_time(): return functools.reduce(lax.psum, axes, x)  39.6 us
    all_gather x1, blocking collectives, side_by_side(): out, at, outs = (lax.all_gather(both, axis, axis=dim, tiled=True), 0, [])  22.7 us
    all_gather x1, waiting for transfers between devices, shards(): block_rows = lax.all_gather(hidden_state, 'tp', axis=0, tiled=True)  14.9 us
    all_to_all x1, starting transfers between devices, sent_to_all(): lax.all_to_all(jnp.broadcast_to(x[None], (peers, *x.shape)), axis, 0, 0,...  7.64 us
    reduce_sum x1, other arithmetic, shards(): jnp.sum(ctx_exp, axis=-1, keepdims=True)  3.82 us
  transfers between devices with their start and end apart: 4, of which 1 were waited for; matrix products, arithmetic and copies ran while one was open for 11% of the time, Pallas kernels for 0%

commit v1 on v0

--- a/solution.py
+++ b/solution.py
@@ -3,6 +3,8 @@
 import jax
 import jax.numpy as jnp
 from jax import lax
+from jax.experimental import pallas as pl
+from jax.experimental.pallas import tpu as pltpu
 from jax.sharding import Mesh
 from jax.sharding import PartitionSpec as P
 
@@ -11,25 +13,341 @@
 HEAD_DIM = 128
 WINDOW_REACH = 128
 GRID_W = 64
-SP = ("sp_0", "sp_1")
-SP_TP = ("sp_0", "sp_1", "tp")
-
+SP = ("z", "y")
+TP = ("x", "c")
+ALL = ("z", "y", "x", "c")
+MESH = pl.DeviceIdType.MESH
 
 NORM_EPS = 1e-05
 MASKED_SCORE = -1e30
-
-
-def one_axis_at_a_time(x, axes):
-    return functools.reduce(lax.psum, axes, x)
-
-
-def side_by_side(arrays, axis, dim, along):
-    both = jnp.concatenate(arrays, axis=along)
-    out, at, outs = (lax.all_gather(both, axis, axis=dim, tiled=True), 0, [])
-    for a in arrays:
-        outs.append(lax.slice_in_dim(out, at, at + a.shape[along], axis=along))
-        at += a.shape[along]
-    return tuple(outs)
+NZ, NY, NX, NC = 16, 4, 4, 2
+F32 = jnp.float32
+BF16 = jnp.bfloat16
+
+
+def wrap(value, size):
+    return lax.rem(value + size, size)
+
+
+def remote(src, dst, send, recv, device):
+    return pltpu.make_async_remote_copy(
+        src_ref=src,
+        dst_ref=dst,
+        send_sem=send,
+        recv_sem=recv,
+        device_id=device,
+        device_id_type=MESH,
+    )
+
+
+def greet(peers):
+    barrier = pltpu.get_barrier_semaphore()
+    for peer in peers:
+        pl.semaphore_signal(barrier, inc=1, device_id=peer, device_id_type=MESH)
+    return lambda: pl.semaphore_wait(barrier, len(peers))
+
+
+def norm_rows(rows, gain, shift, scale):
+    floats = rows.astype(F32)
+    mean = jnp.mean(floats * floats, axis=-1, keepdims=True)
+    normed = floats * lax.rsqrt(mean + NORM_EPS) * gain
+    return (normed * (1.0 + scale) + shift).astype(BF16)
+
+
+def gather_kernel(
+    lat_ref, ctx_ref, gain_ref, cond_ref, cctx_ref, shift_ref, scale_ref, gate_ref,
+    hid_ref, ctxh_ref, mod_ref,
+    rows, parts, ybuf, zsrc, zbuf, gsrc, gbuf,
+    y_send, y_recv, z_send, z_recv, g_send, g_recv, a_send, a_recv, p_send, p_recv,
+):
+    z, y, x, c = (lax.axis_index(a) for a in ALL)
+    tp = x * NC + c
+    right, left = wrap(x + 1, NX), wrap(x - 1, NX)
+    opposite = wrap(x + 2, NX)
+    plane = [
+        (dy, dx, dc)
+        for dy in range(NY)
+        for dx in range(NX)
+        for dc in range(NC)
+        if (dy, dx, dc) != (0, 0, 0)
+    ]
+
+    def plane_peer(dy, dx, dc):
+        return {"y": wrap(y + dy, NY), "x": wrap(x + dx, NX), "c": wrap(c + dc, NC)}
+
+    entered = greet(
+        [plane_peer(*p) for p in plane] + [{"z": wrap(z + d, NZ)} for d in range(1, NZ)]
+    )
+
+    row = lax.broadcasted_iota(jnp.int32, (8, 32), 0)
+    vectors = jnp.where(
+        row == 0,
+        jnp.broadcast_to(cond_ref[...], (8, 32)),
+        jnp.broadcast_to(cctx_ref[...], (8, 32)),
+    )
+    active = (vectors / (1.0 + jnp.exp(-vectors))).astype(BF16)
+    shift_part = jnp.dot(active, shift_ref[...], preferred_element_type=F32)
+    scale_part = jnp.dot(active, scale_ref[...], preferred_element_type=F32)
+    gate_part = jnp.dot(active, gate_ref[...], preferred_element_type=F32)
+    for t in range(2):
+        cols = slice(t * 128, t * 128 + 128)
+        parts[t] = jnp.concatenate(
+            [shift_part[0:1, cols], scale_part[0:1, cols], gate_part[0:1, cols], gate_part[0:1, cols]],
+            axis=0,
+        )
+        parts[2 + t] = jnp.concatenate(
+            [shift_part[1:2, cols], scale_part[1:2, cols], scale_part[1:2, cols], scale_part[1:2, cols]],
+            axis=0,
+        )
+    rows[tp] = lat_ref[...]
+
+    entered()
+
+    half = (pl.ds(0, 48), pl.ds(48, 48))
+    partner = {"c": 1 - c}
+    y_copies = []
+    for d in range(1, NY):
+        target = wrap(y + d, NY)
+        copy = remote(parts.at[target], ybuf.at[d], y_send.at[d], y_recv.at[d], {"y": target})
+        copy.start()
+        y_copies.append(copy)
+    sent = []
+
+    def send_half(owner, h, to, k):
+        source = lat_ref.at[half[h]] if owner is None else rows.at[owner, half[h]]
+        slot = rows.at[tp if owner is None else owner, half[h]]
+        copy = remote(source, slot, a_send.at[k], a_recv.at[k], {"x": to})
+        copy.start()
+        sent.append(copy)
+
+    def send_partner(owner, h, k):
+        if owner is None:
+            copy = remote(lat_ref, rows.at[tp], p_send.at[k], p_recv.at[k], partner)
+        else:
+            copy = remote(
+                rows.at[owner, half[h]], rows.at[owner, half[h]], p_send.at[k], p_recv.at[k], partner
+            )
+        copy.start()
+        sent.append(copy)
+
+    from_left, from_right = left * NC + c, right * NC + c
+    from_opposite = opposite * NC + c
+
+    def arrived(owner, h, k):
+        slot = rows.at[owner, half[h]]
+        remote(slot, slot, a_send.at[k], a_recv.at[k], {"x": right}).wait_recv()
+
+    send_half(None, 0, right, 0)
+    send_half(None, 1, left, 1)
+    send_half(None, 1, right, 2)
+    send_half(None, 0, left, 3)
+    send_partner(None, 0, 0)
+
+    for copy in y_copies:
+        copy.wait_recv()
+    zsrc[...] = parts[y] + ybuf[1] + ybuf[2] + ybuf[3]
+
+    arrived(from_left, 0, 0)
+    send_half(from_left, 0, right, 4)
+    send_partner(from_left, 0, 1)
+    z_copies = []
+    for d in range(1, NZ):
+        copy = remote(zsrc, zbuf.at[d], z_send.at[d], z_recv.at[d], {"z": wrap(z + d, NZ)})
+        copy.start()
+        z_copies.append(copy)
+    arrived(from_right, 1, 1)
+    send_half(from_right, 1, left, 5)
+    send_partner(from_right, 1, 2)
+
+    for copy in z_copies:
+        copy.wait_recv()
+    total = zsrc[...]
+    for d in range(1, NZ):
+        total = total + zbuf[d]
+    gsrc[...] = total
+    gbuf[tp, y] = total
+    arrived(from_left, 1, 2)
+    send_partner(from_left, 1, 3)
+    arrived(from_right, 0, 3)
+    send_partner(from_right, 0, 4)
+    g_copies = []
+    for k, p in enumerate(plane):
+        copy = remote(gsrc, gbuf.at[tp, y], g_send.at[k], g_recv.at[k], plane_peer(*p))
+        copy.start()
+        g_copies.append(copy)
+    arrived(from_opposite, 0, 4)
+    send_partner(from_opposite, 0, 5)
+    arrived(from_opposite, 1, 5)
+    send_partner(from_opposite, 1, 6)
+    for copy in g_copies:
+        copy.wait_recv()
+    for owner in range(NX * NC):
+        for t in range(2):
+            cols = pl.ds((owner * 2 + t) * 128, 128)
+            mod_ref[0:4, cols] = gbuf[owner, t]
+            mod_ref[4:8, cols] = gbuf[owner, 2 + t]
+    ctxh_ref[...] = norm_rows(ctx_ref[...], gain_ref[...], mod_ref[4:5, :], mod_ref[5:6, :])
+    mate = x * NC + 1 - c
+    remote(lat_ref, rows.at[mate], p_send.at[0], p_recv.at[0], partner).wait_recv()
+    others = [(left, 0, 1), (right, 1, 2), (left, 1, 3), (right, 0, 4), (opposite, 0, 5), (opposite, 1, 6)]
+    for chip, h, k in others:
+        slot = rows.at[chip * NC + 1 - c, half[h]]
+        remote(slot, slot, p_send.at[k], p_recv.at[k], partner).wait_recv()
+
+    gain = gain_ref[...]
+    shift = mod_ref[0:1, :]
+    scale = mod_ref[1:2, :]
+
+    def one(i, carry):
+        owner = i // 6
+        part = pl.ds(pl.multiple_of((i % 6) * 16, 16), 16)
+        hid_ref[owner, part] = norm_rows(rows[owner, part], gain, shift, scale)
+        return carry
+
+    lax.fori_loop(0, NX * NC * 6, one, 0)
+    for copy in sent + y_copies + z_copies + g_copies:
+        copy.wait_send()
+
+
+def gathered(latent, context, norm_gain, condition, context_condition, shift_w, scale_w, gate_w):
+    rows, width = latent.shape
+    vmem = pl.BlockSpec(memory_space=pltpu.VMEM)
+    tps = NX * NC
+    return pl.pallas_call(
+        gather_kernel,
+        out_shape=(
+            jax.ShapeDtypeStruct((tps, rows, width), BF16),
+            jax.ShapeDtypeStruct(context.shape, BF16),
+            jax.ShapeDtypeStruct((8, width), F32),
+        ),
+        in_specs=[vmem] * 8,
+        out_specs=(vmem,) * 3,
+        scratch_shapes=[
+            pltpu.VMEM((tps, rows, width), BF16),
+            pltpu.VMEM((4, 4, 128), F32),
+            pltpu.VMEM((NY, 4, 128), F32),
+            pltpu.VMEM((4, 128), F32),
+            pltpu.VMEM((NZ, 4, 128), F32),
+            pltpu.VMEM((4, 128), F32),
+            pltpu.VMEM((tps, NY, 4, 128), F32),
+            pltpu.SemaphoreType.DMA((NY,)),
+            pltpu.SemaphoreType.DMA((NY,)),
+            pltpu.SemaphoreType.DMA((NZ,)),
+            pltpu.SemaphoreType.DMA((NZ,)),
+            pltpu.SemaphoreType.DMA((31,)),
+            pltpu.SemaphoreType.DMA((31,)),
+            pltpu.SemaphoreType.DMA((6,)),
+            pltpu.SemaphoreType.DMA((6,)),
+            pltpu.SemaphoreType.DMA((7,)),
+            pltpu.SemaphoreType.DMA((7,)),
+        ],
+        compiler_params=pltpu.CompilerParams(
+            collective_id=0, has_side_effects=True, vmem_limit_bytes=40 * 1024 * 1024
+        ),
+        cost_estimate=pl.CostEstimate(flops=10**9, bytes_accessed=10**7, transcendentals=0),
+        name="gather",
+    )(
+        latent, context, norm_gain.reshape(1, -1), condition.reshape(1, -1),
+        context_condition.reshape(1, -1), shift_w, scale_w, gate_w,
+    )
+
+
+def output_kernel(
+    att_ref, wo_ref, lat_ref, mod_ref, out_ref,
+    wo_mate, att_mate, opp_src, right_src, left_src, opp_left, opp_right, from_left, from_right,
+    m_send, m_recv, s_send, s_recv,
+):
+    x, c = lax.axis_index("x"), lax.axis_index("c")
+    right, left = wrap(x + 1, NX), wrap(x - 1, NX)
+    entered = greet([{"x": right}, {"x": left}, {"c": 1 - c}])
+    entered()
+    partner = {"c": 1 - c}
+    mates = [remote(wo_ref, wo_mate, m_send.at[4], m_recv.at[4], partner)]
+    for chip in range(NX):
+        mates.append(
+            remote(att_ref.at[chip * NC + 1 - c], att_mate.at[chip], m_send.at[chip], m_recv.at[chip], partner)
+        )
+    for copy in mates:
+        copy.start()
+    for copy in mates:
+        copy.wait_recv()
+
+    def product(chip, h):
+        cols = slice(h * 1024, h * 1024 + 1024)
+        return jnp.dot(
+            att_ref[chip * NC + c], wo_ref[:, cols], preferred_element_type=F32
+        ) + jnp.dot(att_mate[chip], wo_mate[:, cols], preferred_element_type=F32)
+
+    sent = []
+
+    def send(src, dst, k, to):
+        copy = remote(src, dst, s_send.at[k], s_recv.at[k], {"x": to})
+        copy.start()
+        sent.append(copy)
+        return copy
+
+    across = wrap(x + 2, NX)
+    opp_src[0] = product(across, 0).astype(BF16)
+    first_left = send(opp_src.at[0], opp_left, 0, right)
+    opp_src[1] = product(across, 1).astype(BF16)
+    first_right = send(opp_src.at[1], opp_right, 1, left)
+    right_src[1] = product(right, 1).astype(BF16)
+    a = send(right_src.at[1], from_left.at[1], 2, right)
+    left_src[0] = product(left, 0).astype(BF16)
+    b = send(left_src.at[0], from_right.at[0], 3, left)
+    right_part = product(right, 0)
+    first_left.wait_recv()
+    right_src[0] = (right_part + opp_left[...].astype(F32)).astype(BF16)
+    d = send(right_src.at[0], from_left.at[0], 4, right)
+    left_part = product(left, 1)
+    first_right.wait_recv()
+    left_src[1] = (left_part + opp_right[...].astype(F32)).astype(BF16)
+    e = send(left_src.at[1], from_right.at[1], 5, left)
+    a.wait_recv()
+    b.wait_recv()
+    d.wait_recv()
+    e.wait_recv()
+    for h in range(2):
+        cols = slice(h * 1024, h * 1024 + 1024)
+        total = product(x, h) + from_left[h].astype(F32) + from_right[h].astype(F32)
+        out_ref[:, cols] = (
+            lat_ref[:, cols].astype(F32) + mod_ref[2:3, cols] * total
+        ).astype(BF16)
+    for copy in mates + sent:
+        copy.wait_send()
+
+
+def projected_out(attended, out_weight, latent, mod):
+    rows, width = latent.shape
+    vmem = pl.BlockSpec(memory_space=pltpu.VMEM)
+    tps = NX * NC
+    half = width // 2
+    return pl.pallas_call(
+        output_kernel,
+        out_shape=jax.ShapeDtypeStruct((rows, width), BF16),
+        in_specs=[vmem] * 4,
+        out_specs=vmem,
+        scratch_shapes=[
+            pltpu.VMEM(out_weight.shape, BF16),
+            pltpu.VMEM((NX, rows, attended.shape[1]), BF16),
+            pltpu.VMEM((2, rows, half), BF16),
+            pltpu.VMEM((2, rows, half), BF16),
+            pltpu.VMEM((2, rows, half), BF16),
+            pltpu.VMEM((rows, half), BF16),
+            pltpu.VMEM((rows, half), BF16),
+            pltpu.VMEM((2, rows, half), BF16),
+            pltpu.VMEM((2, rows, half), BF16),
+            pltpu.SemaphoreType.DMA((5,)),
+            pltpu.SemaphoreType.DMA((5,)),
+            pltpu.SemaphoreType.DMA((6,)),
+            pltpu.SemaphoreType.DMA((6,)),
+        ],
+        compiler_params=pltpu.CompilerParams(
+            collective_id=1, has_side_effects=True, vmem_limit_bytes=40 * 1024 * 1024
+        ),
+        cost_estimate=pl.CostEstimate(flops=10**9, bytes_accessed=10**7, transcendentals=0),
+        name="output",
+    )(attended.reshape(tps, rows, -1), out_weight, latent, mod)
 
 
 def padded_2(block, sides, width):
@@ -59,17 +377,6 @@
 def gathered_copies(x, axis, dim):
     blocks = sent_to_all(x, axis)
     return laid_out(blocks, dim)
-
-
-def in_blocks(x, dim, peers):
-    before, after = (x.shape[:dim], x.shape[dim + 1 :])
-    return jnp.moveaxis(x.reshape(*before, peers, -1, *after), dim, 0)
-
-
-def summed_on_arrival(x, axis, dim):
-    peers = lax.axis_size(axis)
-    blocks = lax.all_to_all(in_blocks(x, dim, peers), axis, 0, 0, tiled=True)
-    return jnp.sum(blocks.astype(jnp.float32), axis=0)
 
 
 def rotate(vectors, position):
@@ -93,14 +400,6 @@
     return turned.reshape(vectors.shape)
 
 
-def modulated_norm(rows_in, norm_gain, shift, scale):
-    floats = rows_in.astype(jnp.float32)
-    normed = (
-        floats * lax.rsqrt(jnp.mean(floats * floats, axis=-1, keepdims=True) + NORM_EPS) * norm_gain
-    )
-    return (normed * (1.0 + scale) + shift).astype(jnp.bfloat16)
-
-
 def shards(
     latent,
     condition,
@@ -116,24 +415,17 @@
     sink_logit_head,
     out_weight,
 ):
-    tp_count = lax.axis_size("tp")
+    tp_count = NX * NC
     group_rows = latent.shape[0] * tp_count
     offset = lax.axis_index(SP) * group_rows
     total_rows = group_rows * lax.axis_size(SP)
-    active = jax.nn.silu(jnp.stack([condition, context_condition])).astype(jnp.bfloat16)
-    shift_part = jnp.dot(active, shift_weight, preferred_element_type=jnp.float32)
-    scale_part = jnp.dot(active, scale_weight, preferred_element_type=jnp.float32)
-    gate_part = jnp.dot(active[:1], gate_weight, preferred_element_type=jnp.float32)
-    shift_sum, scale_sum, gate_sum = (
-        one_axis_at_a_time(shift_part, SP),
-        one_axis_at_a_time(scale_part, SP),
-        one_axis_at_a_time(gate_part, SP),
-    )
-    shift_all, scale_all, gate_all = side_by_side((shift_sum, scale_sum, gate_sum), "tp", 1, 0)
-    hidden_state = modulated_norm(latent, norm_gain, shift_all[0], scale_all[0])
+    hidden, ctx_hidden, mod = gathered(
+        latent, context, norm_gain, condition, context_condition,
+        shift_weight, scale_weight, gate_weight,
+    )
     query_width = query_weight.shape[1]
     pair_width = key_matrix.shape[1]
-    block_rows = lax.all_gather(hidden_state, "tp", axis=0, tiled=True)
+    block_rows = hidden.reshape(group_rows, -1)
     row_count = block_rows.shape[0]
     position = offset + jnp.arange(row_count, dtype=jnp.int32)
     query_row_block = jnp.dot(block_rows, query_weight, preferred_element_type=jnp.float32)
@@ -150,7 +442,6 @@
         axis=1,
     ).astype(jnp.bfloat16)
     padded = padded_2(projected[:, query_width:], ((SP, 0),), WINDOW_REACH)
-    ctx_hidden = modulated_norm(context, norm_gain, shift_all[1], scale_all[1])
     ctx_pairs = gathered_copies(
         jnp.concatenate(
             [
@@ -221,34 +512,29 @@
         "nhgqc,chd->nqhgd", ctx_weights, context_value_rows, preferred_element_type=jnp.float32
     )
     attended = attended.astype(jnp.bfloat16).reshape(group_rows, query_width)
-    mixed_sum = summed_on_arrival(
-        jnp.dot(attended, out_weight, preferred_element_type=jnp.float32).astype(jnp.bfloat16),
-        "tp",
-        0,
-    )
-    return (latent.astype(jnp.float32) + gate_all[0] * mixed_sum).astype(jnp.bfloat16)
+    return projected_out(attended, out_weight, latent, mod)
 
 
 def solution(mesh):
-    torus = Mesh(mesh.devices.reshape(16, 4, mesh.shape["tp"]), ("sp_0", "sp_1", "tp"))
+    torus = Mesh(mesh.devices.reshape(NZ, NY, NX, NC), ALL)
     return jax.shard_map(
         shards,
         mesh=torus,
         in_specs=(
-            P(SP_TP, None),
+            P(ALL, None),
             P(SP),
             P(SP),
             P(SP, None),
             P(),
-            P(SP, "tp"),
-            P(SP, "tp"),
-            P(SP, "tp"),
-            P(None, "tp"),
-            P(None, "tp"),
-            P(None, "tp"),
-            P("tp"),
-            P("tp", None),
+            P(SP, TP),
+            P(SP, TP),
+            P(SP, TP),
+            P(None, TP),
+            P(None, TP),
+            P(None, TP),
+            P(TP),
+            P(TP, None),
         ),
-        out_specs=P(SP_TP, None),
+        out_specs=P(ALL, None),
         check_vma=False,
     )

time: 189 us -> 138 us (0.73)
  blocking collectives: 105 us -> 0 us
  Pallas kernels: 0 us -> 68.2 us
  between operations: 13.8 us -> 0.31 us
  other arithmetic: 15.8 us -> 6.59 us
  local copies, waits for them, and re-layouts: 5.96 us -> 14 us
  matrix products: 19.8 us -> 12.9 us
  starting transfers between devices: 12.2 us -> 18.1 us
  waiting for transfers between devices: 14.9 us -> 17.7 us
    pallas_call x0 -> x2, Pallas kernels: none -> 68.2 us  [the longest x1 43.4 us: gathered(): pl.pallas_call(gather_kernel, out_shape=(jax.ShapeDtypeStruct((tps, rows,...]
    all_to_all x1 -> x0, blocking collectives: 42.9 us -> none  [summed_on_arrival(): blocks = lax.all_to_all(in_blocks(x, dim, peers), axis, 0, 0, tiled=True)]
    psum x2 -> x0, blocking collectives: 39.6 us -> none  [one_axis_at_a_time(): return functools.reduce(lax.psum, axes, x)]
    all_gather x1 -> x0, blocking collectives: 22.7 us -> none  [side_by_side(): out, at, outs = (lax.all_gather(both, axis, axis=dim, tiled=True), 0, [])]
    all_to_all x1, waiting for transfers between devices: 0.01 us -> 17.7 us  [sent_to_all(): lax.all_to_all(jnp.broadcast_to(x[None], (peers, *x.shape)), axis, 0, 0,...]
    all_gather x1 -> x0, waiting for transfers between devices: 14.9 us -> none  [shards(): block_rows = lax.all_gather(hidden_state, 'tp', axis=0, tiled=True)]
    unnamed x24 -> x35, local copies, waits for them, and re-layouts: 2.13 us -> 10.6 us
    all_to_all x1, starting transfers between devices: 7.64 us -> 14.6 us  [sent_to_all(): lax.all_to_all(jnp.broadcast_to(x[None], (peers, *x.shape)), axis, 0, 0,...]
  transfers between devices with their start and end apart: 4 -> 3, of which waited for: 1 -> 1; matrix products, arithmetic and copies ran while one was open for 11% -> 9% of each run, Pallas kernels for 0% -> 0%
where the time goes in v1:
time: 138 us
  Pallas kernels  68.2 us (49%)
  starting transfers between devices  18.1 us (13%)
  waiting for transfers between devices  17.7 us (13%)
  local copies, waits for them, and re-layouts  14 us (10%)
  matrix products  12.9 us (9%)
  other arithmetic  6.59 us (5%)
    pallas_call x1, Pallas kernels, gathered(): pl.pallas_call(gather_kernel, out_shape=(jax.ShapeDtypeStruct((tps, rows,...  43.4 us
    pallas_call x1, Pallas kernels, projected_out(): pl.pallas_call(output_kernel, out_shape=jax.ShapeDtypeStruct((rows, width...  24.8 us
    all_to_all x1, waiting for transfers between devices, sent_to_all(): lax.all_to_all(jnp.broadcast_to(x[None], (peers, *x.shape)), axis, 0, 0,...  17.7 us
    all_to_all x1, starting transfers between devices, sent_to_all(): lax.all_to_all(jnp.broadcast_to(x[None], (peers, *x.shape)), axis, 0, 0,...  14.6 us
    unnamed x35, local copies, waits for them, and re-layouts  10.6 us
    dot_general x1, matrix products, shards(): jnp.dot(block_rows, query_weight, preferred_element_type=jnp.float32)  3.19 us
    dot_general x1, matrix products, shards(): jnp.dot(block_rows, value_matrix, preferred_element_type=jnp.float32)  2.92 us
  transfers between devices with their start and end apart: 3, of which 1 were waited for; matrix products, arithmetic and copies ran while one was open for 9% of the time, Pallas kernels for 0%

profile of v1, /device:TPU:1, one launch (start us, length us, event | category | flops | bytes accessed | tf_op | source)
XLA Modules:
  0.0 137.8 jit_solution(14343961142347627171)
XLA Ops:
  0.0 1.3 copy.27
  1.4 1.0 copy-done.2
  2.3 0.8 copy-done.4
  3.2 0.7 copy-done.5
  3.9 0.7 copy-done.6
  4.6 0.7 copy-done.7
  5.3 0.7 copy-done.8
  6.0 0.7 copy-done.9
  6.7 0.7 copy-done.10
  7.3 43.4 %gather.1 = (bf16[8,96,2048]{2,1,0:T(8,128)(2,1)S(1)}, bf16[16,2048]{1,0:T(8,128)(2,1)S(1)}, f32[8,2048]{1,0:T(8,128)S(1)}) custom-call(bf16[96,2048]{1,0:T(8,128)(2,1)S(1)} %copy-done.2, bf16[16,2048]{1,0:T(8,128)(2,1)S(1)} %copy-done.4, f32[1,2048]{1,0:T(1,128)S(1)} %bitcast.134, f32[1,32]{1,0:T(1,128)S(1)} %bitcast.135, f32[1,32]{1,0:T(1,128)S(1)} %bitcast.136, ...), custom_call_target="tpu_custom_call" | custom-call | flops 1000000000 | bytes 10000000 | tf_op jit(solution)/shard_map/gather/pallas_call | solution.py:216
  50.8 1.2 convolution_bitcast_fusion.1
  52.5 0.7 subtract_convert_fusion.1
  53.5 2.9 %convolution_convert_fusion = bf16[768,128]{1,0:T(8,128)(2,1)S(1)} fusion(bf16[768,2048]{1,0:T(8,128)(2,1)} %bitcast.138, bf16[2048,128]{1,0:T(8,128)(2,1)S(1)} %copy-done), kind=kOutput, calls=%fused_computation.23 | convolution fusion | flops 402751488 | bytes 3866624 | tf_op jit(solution)/shard_map/dot_general | solution.py:435
  56.4 0.7 pad_maximum_fusion.11
  57.0 2.3 %collective-permute-start = (bf16[128,256]{1,0:T(8,128)(2,1)}, bf16[128,256]{1,0:T(8,128)(2,1)S(1)}, u32[]{:S(2)}, u32[]{:S(2)}) collective-permute-start(bf16[128,256]{1,0:T(8,128)(2,1)} %get-tuple-element.21), channel_id=1, source_target_pairs={{0,8},{8,16},{16,24},{24,32},{32,40},{40,48},{48,56},{56,64},{64,7... | collective-permute-start | bytes 196616 | tf_op jit(solution)/shard_map/ppermute | solution.py:358
  59.3 1.3 collective-permute-start.1
  61.0 0.9 broadcast_in_dim.12
  61.9 14.6 %all-to-all-start = ((bf16[64,16,256]{2,1,0:T(8,128)(2,1)}), bf16[64,16,256]{2,1,0:T(8,128)(2,1)S(1)}, u32[]{:S(2)}, u32[]{:S(2)}) async-start(bf16[64,16,256]{2,1,0:T(8,128)(2,1)} %broadcast_in_dim.12), calls=%async_computation | async-start | bytes 1048576 | tf_op jit(solution)/shard_map/all_to_all | solution.py:368
  76.8 1.4 %copy.33 = bf16[2048,256]{0,1:T(8,128)(2,1)} copy(bf16[2048,256]{1,0:T(8,128)(2,1)S(1)} %copy-done.14) | data formatting | bytes 2097152 | tf_op args[8]
  78.2 0.7 fusion.31
  79.0 1.4 %fusion.18 = pred[6,128,384]{1,2,0:T(8,128)(4,1)S(1)} fusion(s32[6,128]{1,0:T(8,128)S(1)} %iota_add_fusion.1, s32[6,384]{1,0:T(8,128)S(1)} %iota_add_fusion, pred[6,384]{1,0:T(8,128)(4,1)S(1)} %get-tuple-element.30, pred[6,384]{1,0:T(8,128)(4,1)S(1)} %get-tuple-element.29), kind=kLoop, calls=%fused_computation.21 | loop fusion | flops 1474560 | bytes 311808 | tf_op jit(solution)/shard_map/and | solution.py:483
  80.4 3.2 %fusion.50 = f32[768,2,2,2,32]{0,4,3,2,1:T(8,128)S(1)} fusion(bf16[768,2048,1,1,1]{1,0,4,3,2:T(8,128)(2,1)} %bitcast.139, bf16[2,2,2,32,2048]{4,3,2,1,0:T(8,128)(2,1)} %bitcast.144), kind=kOutput, calls=%fused_computation.93 | convolution fusion | flops 805306368 | bytes 4980736 | tf_op jit(solution)/shard_map/dot_general | solution.py:431
  85.0 0.9 pad_maximum_fusion.6
  86.2 1.9 %fusion.6 = (f32[6,2,128]{2,1,0:T(2,128)S(1)}, f32[6,384,128,2]{2,1,3,0:T(8,128)}) fusion(pred[6,128,384]{1,2,0:T(8,128)(4,1)S(1)} %fusion.18, bf16[6,128,2,128]{3,1,2,0:T(8,128)(2,1)S(1)} %copy.34, bf16[6,128,1,128]{3,1,0,2:T(8,128)(2,1)S(1)} %bitcast.149, bf16[6,128,1,128]{3,1,0,2:T(8,128)(2,1)S(1)} %copy.32, bf16[6,128,1,128]{3,1,0,2:T(8,128)(2,1)S(1)} %bitcast.148), kind=kOutput, calls=%fused_computation.12 | convolution fusion | flops 154532352 | bytes 3643392 | tf_op jit(solution)/shard_map/nqhgd,nkhd->nhgqk/dot_general | solution.py:470
  88.1 17.7 %all-to-all-done = bf16[64,16,256]{2,1,0:T(8,128)(2,1)S(1)} async-done(((bf16[64,16,256]{2,1,0:T(8,128)(2,1)}), bf16[64,16,256]{2,1,0:T(8,128)(2,1)S(1)}, u32[]{:S(2)}, u32[]{:S(2)}) %all-to-all-start) | async-done | bytes 524320 | tf_op jit(solution)/shard_map/all_to_all | solution.py:368
  105.8 1.0 bitcast_reduce_fusion
  106.9 1.0 fusion.1
  107.9 0.6 copy-done.12
  109.2 0.8 convolution_bitcast_fusion
  110.0 1.5 %fusion.13 = bf16[6,128,1,2,128]{1,4,3,0,2:T(8,128)(2,1)S(1)} fusion(f32[6,128,1,2,128]{1,4,3,0,2:T(8,128)S(1)} %convolution_bitcast_fusion, f32[6,2,128]{2,1,0:T(2,128)S(1)} %exponential_add_fusion, f32[6,2,128]{2,1,0:T(2,128)S(1)} %maximum_maximum_fusion, f32[1024,6,128,2]{2,0,3,1:T(8,128)S(1)} %get-tuple-element.36, bf16[1024,256]{1,0:T(8,128)(2,1)S(1)} %bitcast.143), kind=kOutput, calls=%fused_computation.16 | convolution fusion | flops 409337856 | bytes 7745536 | tf_op jit(solution)/shard_map/nhgqc,chd->nqhgd/dot_general | solution.py:511
  112.2 24.8 %output.1 = bf16[96,2048]{1,0:T(8,128)(2,1)S(1)} custom-call(bf16[8,96,256]{2,1,0:T(8,128)(2,1)S(1)} %reshape_reshape.12.att_ref, bf16[256,2048]{1,0:T(8,128)(2,1)S(1)} %copy-done.1, bf16[96,2048]{1,0:T(8,128)(2,1)S(1)} %copy-done.3, f32[8,2048]{1,0:T(8,128)S(1)} %get-tuple-element.10.mod_ref), custom_call_target="tpu_custom_call" | custom-call | flops 1000000000 | bytes 10000000 | tf_op jit(solution)/shard_map/output/pallas_call | solution.py:325
  137.0 0.7 copy.50
  (51 shorter events, 4.7 us)
Async XLA Ops:
  0.0 53.4 %copy-start = (bf16[2048,128]{1,0:T(8,128)(2,1)S(1)}, bf16[2048,128]{1,0:T(8,128)(2,1)}, u32[]{:S(2)}) copy-start(bf16[2048,128]{1,0:T(8,128)(2,1)} %param.23) | copy-start | bytes 1572868
  1.3 1.0 copy-start.2
  2.3 0.8 copy-start.4
  3.2 0.7 copy-start.5
  3.9 0.7 copy-start.6
  4.6 0.7 copy-start.7
  5.3 0.7 copy-start.8
  6.0 0.7 copy-start.9
  6.7 0.7 copy-start.10
  50.7 1.7 %copy-start.11 = (bf16[8,96,2048]{2,1,0:T(8,128)(2,1)}, bf16[8,96,2048]{2,1,0:T(8,128)(2,1)S(1)}, u32[]{:S(2)}) copy-start(bf16[8,96,2048]{2,1,0:T(8,128)(2,1)S(1)} %get-tuple-element.8) | copy-start | bytes 9437188
  53.4 7.4 %copy-start.13 = (bf16[2048,128]{1,0:T(8,128)(2,1)S(1)}, bf16[2048,128]{1,0:T(8,128)(2,1)}, u32[]{:S(2)}) copy-start(bf16[2048,128]{1,0:T(8,128)(2,1)} %param.22) | copy-start | bytes 1572868
  56.4 20.4 %copy-start.14 = (bf16[2048,256]{1,0:T(8,128)(2,1)S(1)}, bf16[2048,256]{1,0:T(8,128)(2,1)}, u32[]{:S(2)}) copy-start(bf16[2048,256]{1,0:T(8,128)(2,1)} %param.21) | copy-start | bytes 3145732
  57.0 27.9 %collective-permute-start = (bf16[128,256]{1,0:T(8,128)(2,1)}, bf16[128,256]{1,0:T(8,128)(2,1)S(1)}, u32[]{:S(2)}, u32[]{:S(2)}) collective-permute-start(bf16[128,256]{1,0:T(8,128)(2,1)} %get-tuple-element.21), channel_id=1, source_target_pairs={{0,8},{8,16},{16,24},{24,32},{32,40},{40,48},{48,56},{56,64},{64,7... | collective-permute-start | bytes 196616 | tf_op jit(solution)/shard_map/ppermute | solution.py:358
  59.3 25.6 %collective-permute-start.1 = (bf16[128,256]{1,0:T(8,128)(2,1)}, bf16[128,256]{1,0:T(8,128)(2,1)}, u32[]{:S(2)}, u32[]{:S(2)}) collective-permute-start(bf16[128,256]{1,0:T(8,128)(2,1)} %get-tuple-element.22), channel_id=1, source_target_pairs={{8,0},{16,8},{24,16},{32,24},{40,32},{48,40},{56,48},{64,56},{72,6... | collective-permute-start | bytes 196616 | tf_op jit(solution)/shard_map/ppermute | solution.py:361
  61.9 43.9 %all-to-all-start = ((bf16[64,16,256]{2,1,0:T(8,128)(2,1)}), bf16[64,16,256]{2,1,0:T(8,128)(2,1)S(1)}, u32[]{:S(2)}, u32[]{:S(2)}) async-start(bf16[64,16,256]{2,1,0:T(8,128)(2,1)} %broadcast_in_dim.12), calls=%async_computation | async-start | bytes 1048576 | tf_op jit(solution)/shard_map/all_to_all | solution.py:368
  105.8 1.0 copy-start.15
  106.9 1.7 %copy-start.12 = (f32[6,384,128,2]{2,1,3,0:T(8,128)S(1)}, f32[6,384,128,2]{2,1,3,0:T(8,128)}, u32[]{:S(2)}) copy-start(f32[6,384,128,2]{2,1,3,0:T(8,128)} %get-tuple-element.34) | copy-start | bytes 7077892
  110.0 2.2 %copy-start.1 = (bf16[256,2048]{1,0:T(8,128)(2,1)S(1)}, bf16[256,2048]{1,0:T(8,128)(2,1)}, u32[]{:S(2)}) copy-start(bf16[256,2048]{1,0:T(8,128)(2,1)} %wo_ref.1) | copy-start | bytes 3145732
  110.0 2.2 %copy-start.3 = (bf16[96,2048]{1,0:T(8,128)(2,1)S(1)}, bf16[96,2048]{1,0:T(8,128)(2,1)}, u32[]{:S(2)}) copy-start(bf16[96,2048]{1,0:T(8,128)(2,1)} %lat_ref.3) | copy-start | bytes 1179652

commit v2 on v0

v2 whole, which is shorter than its diff:
```python
import functools

import jax
import jax.numpy as jnp
import numpy as np
from jax import lax
from jax.experimental import pallas as pl
from jax.experimental.pallas import tpu as pltpu
from jax.sharding import Mesh
from jax.sharding import PartitionSpec as P

HEAD_DIM = 128
WINDOW_REACH = 128
GRID_W = 64
SP = ("z", "y")
TP = ("x", "c")
ALL = ("z", "y", "x", "c")
MESH = pl.DeviceIdType.MESH

NORM_EPS = 1e-05
MASKED_SCORE = -1e30
LOG2E = 1.4426950408889634
NZ, NY, NX, NC = 16, 4, 4, 2
NTP = NX * NC
WIDTH = 2048
ROWS = 96
GROUP = ROWS * NTP
CHIP = ROWS * NC
CTX_ROWS = 16
WIN = 512
F32 = jnp.float32
BF16 = jnp.bfloat16
PLANE = [
    (dy, dx, dc)
    for dy in range(NY)
    for dx in range(NX)
    for dc in range(NC)
    if (dy, dx, dc) != (0, 0, 0)
]


def wrap(value, size):
    return lax.rem(value + size, size)


def remote(src, dst, send, recv, device):
    return pltpu.make_async_remote_copy(
        src_ref=src,
        dst_ref=dst,
        send_sem=send,
        recv_sem=recv,
        device_id=device,
        device_id_type=MESH,
    )


def rows_at(start, count):
    return pl.ds(pl.multiple_of(start, 16), count)


def block_kernel(
    lat_hbm, ctx_hbm, gain_hbm, cond_hbm, cctx_hbm, sw_hbm, cw_hbm, gw_hbm,
    wq_hbm, wk_hbm, wv_hbm, sink_hbm, wo_hbm, freq_hbm,
    out_ref,
    lat, ctx, gain, cond, cctx, sw, cw, gw, wqkv, sink, wo, freq,
    rows, parts, ybuf, zsrc, zbuf, gsrc, gbuf, mod, amp, camp,
    cos_t, sin_t, band, hid, qkv, q, kv, ctxkv,
    att, att_mate, wo_mate, opp_src, right_src, left_src, opp_left, opp_right, from_left, from_right,
    l_sem, y_send, y_recv, z_send, z_recv, g_send, g_recv, a_send, a_recv, p_send, p_recv,
    c_send, c_recv, d_send, d_recv, h_send, h_recv, m_send, m_recv, s_send, s_recv,
):
    z, y, x, c = (lax.axis_index(a) for a in ALL)
    tp = x * NC + c
    sp = z * NY + y
    right, left, across = wrap(x + 1, NX), wrap(x - 1, NX), wrap(x + 2, NX)
    up, down = wrap(y + 1, NY), wrap(y - 1, NY)
    partner = {"c": 1 - c}
    after = {"z": wrap(z + (y + 1) // NY, NZ), "y": up}
    before = {"z": wrap(z - (NY - y) // NY, NZ), "y": down}

    def plane_peer(dy, dx, dc):
        return {"y": wrap(y + dy, NY), "x": wrap(x + dx, NX), "c": wrap(c + dc, NC)}

    barrier = pltpu.get_barrier_semaphore()
    peers = [{"z": wrap(z + d, NZ)} for d in range(1, NZ)]
    peers += [plane_peer(*p) for p in PLANE] + [after, before]
    for peer in peers:
        pl.semaphore_signal(barrier, inc=1, device_id=peer, device_id_type=MESH)
    pairs = [
        (cond_hbm, cond), (cctx_hbm, cctx), (sw_hbm, sw), (cw_hbm, cw), (gw_hbm, gw),
        (lat_hbm, lat), (freq_hbm, freq), (ctx_hbm, ctx), (gain_hbm, gain), (sink_hbm, sink),
        (wq_hbm, wqkv.at[:, pl.ds(0, 256)]), (wk_hbm, wqkv.at[:, pl.ds(256, 128)]),
        (wv_hbm, wqkv.at[:, pl.ds(384, 128)]), (wo_hbm, wo),
        (lat_hbm, rows.at[rows_at(tp * ROWS, ROWS)]),
    ]
    local = [pltpu.make_async_copy(s, d, l_sem.at[k]) for k, (s, d) in enumerate(pairs)]
    for copy in local:
        copy.start()

    for copy in local[:5]:
        copy.wait()
    row = lax.broadcasted_iota(jnp.int32, (8, 32), 0)
    vectors = jnp.where(
        row == 0, jnp.broadcast_to(cond[...], (8, 32)), jnp.broadcast_to(cctx[...], (8, 32))
    )
    active = (vectors / (1.0 + jnp.exp(-vectors))).astype(BF16)
    shift_part = jnp.dot(active, sw[...], preferred_element_type=F32)
    scale_part = jnp.dot(active, cw[...], preferred_element_type=F32)
    gate_part = jnp.dot(active, gw[...], preferred_element_type=F32)
    for t in range(2):
        cols = slice(t * 128, t * 128 + 128)
        parts[t] = jnp.concatenate(
            [shift_part[0:1, cols], scale_part[0:1, cols], gate_part[0:1, cols], gate_part[0:1, cols]],
            axis=0,
        )
        parts[2 + t] = jnp.concatenate(
            [shift_part[1:2, cols], scale_part[1:2, cols], scale_part[1:2, cols], scale_part[1:2, cols]],
            axis=0,
        )
    for copy in local[5:]:
        copy.wait()
    pl.semaphore_wait(barrier, len(peers))

    sent = []

    def send(src, dst, s_sem, r_sem, k, to):
        copy = remote(src, dst, s_sem.at[k], r_sem.at[k], to)
        copy.start()
        sent.append(copy)
        return copy

    y_copies = [
        send(parts.at[wrap(y + d, NY)], ybuf.at[d], y_send, y_recv, d, {"y": wrap(y + d, NY)})
        for d in range(1, NY)
    ]

    def piece(chip, core, h):
        return rows.at[rows_at((chip * NC + core) * ROWS + h * 48, 48)]

    def along(chip, h, k, to):
        source = lat.at[pl.ds(h * 48, 48)] if chip is None else piece(chip, c, h)
        slot = piece(x if chip is None else chip, c, h)
        send(source, slot, a_send, a_recv, k, {"x": to})

    def across_chip(chip, h, k):
        send(piece(chip, c, h), piece(chip, c, h), p_send, p_recv, k, partner)

    def arrived(chip, h, k):
        slot = piece(chip, c, h)
        remote(slot, slot, a_send.at[k], a_recv.at[k], {"x": right}).wait_recv()

    along(None, 0, 0, right)
    along(None, 1, 1, left)
    along(None, 1, 2, right)
    along(None, 0, 3, left)
    own_slot = rows.at[rows_at(tp * ROWS, ROWS)]
    send(lat, own_slot, p_send, p_recv, 0, partner)
    send(wo, wo_mate, m_send, m_recv, 4, partner)

    for copy in y_copies:
        copy.wait_recv()
    zsrc[...] = parts[y] + ybuf[1] + ybuf[2] + ybuf[3]

    lane = lax.broadcasted_iota(jnp.int32, (64, 128), 1)
    sign = jnp.where(lane % 64 < 32, -1.0, 1.0)
    col_angle = lax.broadcasted_iota(jnp.int32, (64, 128), 0).astype(F32) * freq[...]
    col_cos, col_sin = jnp.cos(col_angle), jnp.sin(col_angle) * sign
    row_ids = sp * (GROUP // GRID_W) + lax.broadcasted_iota(jnp.int32, (16, 128), 0)
    row_angle = row_ids.astype(F32) * freq[...]
    row_cos, row_sin = jnp.cos(row_angle), jnp.sin(row_angle) * sign[0:16]

    z_copies = [
        send(zsrc, zbuf.at[d], z_send, z_recv, d, {"z": wrap(z + d, NZ)})
        for d in (8, 7, 9, 6, 10, 5, 11, 4, 12, 3, 13, 2, 14, 1, 15)
    ]
    for i in range(GROUP // GRID_W):
        block = slice(i * GRID_W, i * GRID_W + GRID_W)
        cos_t[block] = jnp.where(lane < 64, jnp.broadcast_to(row_cos[i : i + 1], (64, 128)), col_cos)
        sin_t[block] = jnp.where(lane < 64, jnp.broadcast_to(row_sin[i : i + 1], (64, 128)), col_sin)
    gap = lax.broadcasted_iota(jnp.int32, (CHIP, WIN), 1) - lax.broadcasted_iota(
        jnp.int32, (CHIP, WIN), 0
    )
    band[...] = jnp.where((gap >= 0) & (gap <= 2 * WINDOW_REACH), 0.0, MASKED_SCORE)
    kv[1024:, :] = jnp.zeros((64, 256), BF16)

    arrived(left, 0, 0)
    along(left, 0, 4, right)
    across_chip(left, 0, 1)
    arrived(right, 1, 1)
    along(right, 1, 5, left)
    across_chip(right, 1, 2)

    for copy in z_copies:
        copy.wait_recv()
    total = zsrc[...]
    for d in range(1, NZ):
        total = total + zbuf[d]
    gsrc[...] = total
    gbuf[tp, y] = total
    g_copies = [
        send(gsrc, gbuf.at[tp, y], g_send, g_recv, k, plane_peer(*p)) for k, p in enumerate(PLANE)
    ]
    arrived(left, 1, 2)
    across_chip(left, 1, 3)
    arrived(right, 0, 3)
    across_chip(right, 0, 4)
    for copy in g_copies:
        copy.wait_recv()
    for owner in range(NTP):
        for t in range(2):
            cols = pl.ds((owner * 2 + t) * 128, 128)
            mod[0:4, cols] = gbuf[owner, t]
            mod[4:8, cols] = gbuf[owner, 2 + t]
    amp[...] = gain[...] * (1.0 + mod[1:2, :])
    camp[...] = gain[...] * (1.0 + mod[5:6, :])

    def normed(value, gains, shifts):
        floats = value.astype(F32)
        mean = jnp.mean(floats * floats, axis=-1, keepdims=True)
        return (floats * lax.rsqrt(mean + NORM_EPS) * gains + shifts).astype(BF16)

    ctx_hidden = normed(ctx[...], camp[...], mod[4:5, :])
    ctxkv[0, 0] = jnp.dot(ctx_hidden, wqkv[:, 256:512], preferred_element_type=F32).astype(BF16)
    cz = [
        send(ctxkv.at[0, 0], ctxkv.at[0, d], c_send, c_recv, d, {"z": wrap(z + d, NZ)})
        for d in (8, 7, 9, 6, 10, 5, 11, 4, 12, 3, 13, 2, 14, 1, 15)
    ]
    cz_of = dict(zip((8, 7, 9, 6, 10, 5, 11, 4, 12, 3, 13, 2, 14, 1, 15), cz))

    arrived(across, 0, 4)
    across_chip(across, 0, 5)
    arrived(across, 1, 5)
    across_chip(across, 1, 6)
    remote(lat, rows.at[rows_at((x * NC + 1 - c) * ROWS, ROWS)], p_send.at[0], p_recv.at[0], partner).wait_recv()
    for chip, h, k in [(left, 0, 1), (right, 1, 2), (left, 1, 3), (right, 0, 4), (across, 0, 5), (across, 1, 6)]:
        slot = piece(chip, 1 - c, h)
        remote(slot, slot, p_send.at[k], p_recv.at[k], partner).wait_recv()

    lanes = lax.broadcasted_iota(jnp.int32, (16, 128), 1)
    first = lanes % 64 < 32

    def project(chips):
        for n, chip in enumerate(chips):
            def norm_step(i, carry):
                for g in range(4):
                    src = rows_at(chip * CHIP + i * 64 + g * 16, 16)
                    dst = rows_at(n * CHIP + i * 64 + g * 16, 16)
                    acc = jnp.zeros((16, 128), F32)
                    for j in range(WIDTH // 128):
                        v = rows[src, j * 128 : j * 128 + 128].astype(F32)
                        acc = acc + v * v
                    mean = jnp.sum(acc, axis=1, keepdims=True) * (1.0 / WIDTH)
                    inverse = jnp.broadcast_to(lax.rsqrt(mean + NORM_EPS), (16, 128))
                    for j in range(WIDTH // 128):
                        cols = slice(j * 128, j * 128 + 128)
                        v = rows[src, cols].astype(F32)
                        hid[dst, cols] = (v * inverse * amp[:, cols] + mod[0:1, cols]).astype(BF16)
                return carry

            lax.fori_loop(0, CHIP // 64, norm_step, 0)
        qkv[...] = jnp.dot(hid[...], wqkv[...], preferred_element_type=F32)
        for n, chip in enumerate(chips):
            def turn_step(i, carry):
                for g in range(2):
                    at = rows_at(n * CHIP + i * 32 + g * 16, 16)
                    to = rows_at(chip * CHIP + i * 32 + g * 16, 16)
                    pad = rows_at(chip * CHIP + i * 32 + g * 16 + WINDOW_REACH, 16)
                    cosine, sine = cos_t[to], sin_t[to]
                    for h in range(3):
                        u = qkv[at, h * 128 : h * 128 + 128]
                        swapped = jnp.where(first, pltpu.roll(u, 96, 1), pltpu.roll(u, 32, 1))
                        turned = (u * cosine + swapped * sine).astype(BF16)
                        if h < 2:
                            q[to, h * 128 : h * 128 + 128] = turned
                        else:
                            kv[pad, 0:128] = turned
                    kv[pad, 128:256] = qkv[at, 384:512].astype(BF16)
                return carry

            lax.fori_loop(0, CHIP // 32, turn_step, 0)

    project((0, 3))
    halo = [
        send(kv.at[pl.ds(GROUP, 128)], kv.at[pl.ds(0, 128)], h_send, h_recv, 0, after),
        send(kv.at[pl.ds(128, 128)], kv.at[pl.ds(GROUP + 128, 128)], h_send, h_recv, 1, before),
    ]
    for d in range(1, 8):
        cz_of[d].wait_recv()
    send(ctxkv.at[0, pl.ds(0, 8)], ctxkv.at[1, pl.ds(0, 8)], d_send, d_recv, 0, {"y": up})
    send(ctxkv.at[0, pl.ds(0, 8)], ctxkv.at[2, pl.ds(0, 8)], d_send, d_recv, 3, {"y": down})
    for d in range(8, 16):
        cz_of[d].wait_recv()
    send(ctxkv.at[0, pl.ds(8, 8)], ctxkv.at[2, pl.ds(8, 8)], d_send, d_recv, 1, {"y": down})
    send(ctxkv.at[0, pl.ds(8, 8)], ctxkv.at[1, pl.ds(8, 8)], d_send, d_recv, 2, {"y": up})

    project((1, 2))

    def ctx_arrived(slot, h, k):
        ref = ctxkv.at[slot, pl.ds(h * 8, 8)]
        remote(ref, ref, d_send.at[k], d_recv.at[k], {"y": up}).wait_recv()

    ctx_arrived(1, 0, 0)
    send(ctxkv.at[1, pl.ds(0, 8)], ctxkv.at[3, pl.ds(0, 8)], d_send, d_recv, 4, {"y": up})
    ctx_arrived(2, 1, 1)
    send(ctxkv.at[2, pl.ds(8, 8)], ctxkv.at[3, pl.ds(8, 8)], d_send, d_recv, 5, {"y": down})
    for copy in halo:
        copy.wait_recv()
    ctx_arrived(1, 1, 2)
    ctx_arrived(2, 0, 3)
    ctx_arrived(3, 0, 4)
    ctx_arrived(3, 1, 5)

    nt = (((1,), (1,)), ((), ()))
    factor = HEAD_DIM ** (-0.5) * LOG2E
    last = sp * GROUP - WINDOW_REACH

    def attend(chip):
        begin = chip * CHIP
        at = rows_at(begin, CHIP)
        both = jnp.concatenate([q[at, 0:128], q[at, 128:256]], axis=0)
        window = rows_at(begin, WIN)
        key_at = last + begin + lax.broadcasted_iota(jnp.int32, (1, WIN), 1)
        edge = jnp.where((key_at >= 0) & (key_at < GROUP * NZ * NY), 0.0, MASKED_SCORE)
        bias = band[...] + edge
        near = lax.dot_general(both, kv[window, 0:128], nt, preferred_element_type=F32)
        near = near * factor + jnp.concatenate([bias, bias], axis=0)
        keys = ctxkv[:, :, :, 0:128].reshape(1024, 128)
        values = ctxkv[:, :, :, 128:256].reshape(1024, 128)
        far = lax.dot_general(both, keys, nt, preferred_element_type=F32) * factor
        head = lax.broadcasted_iota(jnp.int32, (2 * CHIP, 1), 0)
        sinks = jnp.where(head < CHIP, sink[0:1, 0:1], sink[0:1, 1:2]) * LOG2E
        top = jnp.maximum(
            jnp.maximum(jnp.max(near, axis=1, keepdims=True), jnp.max(far, axis=1, keepdims=True)), sinks
        )
        near = jnp.exp2(near - top)
        far = jnp.exp2(far - top)
        bottom = (
            jnp.sum(near, axis=1, keepdims=True)
            + jnp.sum(far, axis=1, keepdims=True)
            + jnp.exp2(sinks - top)
        )
        mixed = jnp.dot(near.astype(BF16), kv[window, 128:256], preferred_element_type=F32)
        mixed = mixed + jnp.dot(far.astype(BF16), values, preferred_element_type=F32)
        mixed = (mixed / bottom).astype(BF16)
        for h in range(2):
            for core in range(NC):
                begin = h * CHIP + core * ROWS
                att[chip, core, :, h * 128 : h * 128 + 128] = mixed[begin : begin + ROWS]
        return send(att.at[chip, 1 - c], att_mate.at[chip], m_send, m_recv, chip, partner)

    def product(chip, h):
        cols = slice(h * 1024, h * 1024 + 1024)
        return jnp.dot(att[chip, c], wo[:, cols], preferred_element_type=F32) + jnp.dot(
            att_mate[chip], wo_mate[:, cols], preferred_element_type=F32
        )

    def around(src, dst, k, to):
        return send(src, dst, s_send, s_recv, k, {"x": to})

    remote(wo, wo_mate, m_send.at[4], m_recv.at[4], partner).wait_recv()
    attend(across).wait_recv()
    opp_src[0] = product(across, 0).astype(BF16)
    first_left = around(opp_src.at[0], opp_left, 0, right)
    opp_src[1] = product(across, 1).astype(BF16)
    first_right = around(opp_src.at[1], opp_right, 1, left)
    right_mate = attend(right)
    left_mate = attend(left)
    right_mate.wait_recv()
    right_src[1] = product(right, 1).astype(BF16)
    r1 = around(right_src.at[1], from_left.at[1], 2, right)
    left_mate.wait_recv()
    left_src[0] = product(left, 0).astype(BF16)
    l0 = around(left_src.at[0], from_right.at[0], 3, left)
    own_mate = attend(x)
    right_part = product(right, 0)
    first_left.wait_recv()
    right_src[0] = (right_part + opp_left[...].astype(F32)).astype(BF16)
    r0 = around(right_src.at[0], from_left.at[0], 4, right)
    left_part = product(left, 1)
    first_right.wait_recv()
    left_src[1] = (left_part + opp_right[...].astype(F32)).astype(BF16)
    l1 = around(left_src.at[1], from_right.at[1], 5, left)
    own_mate.wait_recv()
    totals = [product(x, h) for h in range(2)]
    for copy in (r1, l0, r0, l1):
        copy.wait_recv()
    for h in range(2):
        cols = slice(h * 1024, h * 1024 + 1024)
        total = totals[h] + from_left[h].astype(F32) + from_right[h].astype(F32)
        out_ref[:, cols] = (lat[:, cols].astype(F32) + mod[2:3, cols] * total).astype(BF16)
    for copy in sent:
        copy.wait_send()


def shards(
    latent,
    condition,
    context_condition,
    context,
    norm_gain,
    shift_weight,
    scale_weight,
    gate_weight,
    query_weight,
    key_matrix,
    value_matrix,
    sink_logit_head,
    out_weight,
):
    lanes = np.arange(HEAD_DIM) % 32
    freq = (10000.0 ** (-(2.0 * lanes) / 64.0)).astype(np.float32)[None]
    vm = pltpu.VMEM
    dma = pltpu.SemaphoreType.DMA
    half = (2, ROWS, WIDTH // 2)
    return pl.pallas_call(
        block_kernel,
        out_shape=jax.ShapeDtypeStruct((ROWS, WIDTH), BF16),
        in_specs=[pl.BlockSpec(memory_space=pl.ANY)] * 14,
        out_specs=pl.BlockSpec(memory_space=pltpu.VMEM),
        scratch_shapes=[
            vm((ROWS, WIDTH), BF16), vm((CTX_ROWS, WIDTH), BF16), vm((1, WIDTH), F32),
            vm((1, 32), F32), vm((1, 32), F32),
            vm((32, 256), BF16), vm((32, 256), BF16), vm((32, 256), BF16),
            vm((WIDTH, 512), BF16), vm((1, 2), F32), vm((256, WIDTH), BF16), vm((1, 128), F32),
            vm((GROUP, WIDTH), BF16),
            vm((4, 4, 128), F32), vm((NY, 4, 128), F32), vm((4, 128), F32), vm((NZ, 4, 128), F32),
            vm((4, 128), F32), vm((NTP, NY, 4, 128), F32),
            vm((8, WIDTH), F32), vm((1, WIDTH), F32), vm((1, WIDTH), F32),
            vm((GROUP, 128), F32), vm((GROUP, 128), F32), vm((CHIP, WIN), F32),
            vm((2 * CHIP, WIDTH), BF16), vm((2 * CHIP, 512), F32),
            vm((GROUP, 256), BF16), vm((GROUP + 256 + 64, 256), BF16),
            vm((NY, NZ, CTX_ROWS, 256), BF16),
            vm((NX, NC, ROWS, 256), BF16), vm((NX, ROWS, 256), BF16), vm((256, WIDTH), BF16),
            vm(half, BF16), vm(half, BF16), vm(half, BF16),
            vm(half[1:], BF16), vm(half[1:], BF16), vm(half, BF16), vm(half, BF16),
            dma((15,)),
            dma((NY,)), dma((NY,)), dma((NZ,)), dma((NZ,)), dma((31,)), dma((31,)),
            dma((6,)), dma((6,)), dma((7,)), dma((7,)),
            dma((NZ,)), dma((NZ,)), dma((6,)), dma((6,)), dma((2,)), dma((2,)),
            dma((5,)), dma((5,)), dma((6,)), dma((6,)),
        ],
        compiler_params=pltpu.CompilerParams(
            collective_id=0, has_side_effects=True, vmem_limit_bytes=62 * 1024 * 1024
        ),
        cost_estimate=pl.CostEstimate(flops=10**9, bytes_accessed=10**7, transcendentals=0),
        name="block",
    )(
        latent, context, norm_gain.reshape(1, -1), condition.reshape(1, -1),
        context_condition.reshape(1, -1), shift_weight, scale_weight, gate_weight,
        query_weight, key_matrix, value_matrix, sink_logit_head.reshape(1, -1), out_weight,
        jnp.asarray(freq),
    )


def solution(mesh):
    torus = Mesh(mesh.devices.reshape(NZ, NY, NX, NC), ALL)
    return jax.shard_map(
        shards,
        mesh=torus,
        in_specs=(
            P(ALL, None),
            P(SP),
            P(SP),
            P(SP, None),
            P(),
            P(SP, TP),
            P(SP, TP),
            P(SP, TP),
            P(None, TP),
            P(None, TP),
            P(None, TP),
            P(TP),
            P(TP, None),
        ),
        out_specs=P(ALL, None),
        check_vma=False,
    )
```

time: 189 us -> 72.8 us (0.39)
  blocking collectives: 105 us -> 0 us
  Pallas kernels: 0 us -> 70.9 us
  matrix products: 19.8 us -> 0 us
  other arithmetic: 15.8 us -> 0 us
  waiting for transfers between devices: 14.9 us -> 0 us
  between operations: 13.8 us -> 0.01 us
  starting transfers between devices: 12.2 us -> 0 us
  local copies, waits for them, and re-layouts: 5.96 us -> 1.77 us
    pallas_call x0 -> x1, Pallas kernels: none -> 70.9 us  [shards(): pl.pallas_call(block_kernel, out_shape=jax.ShapeDtypeStruct((ROWS, WIDTH)...]
    all_to_all x1 -> x0, blocking collectives: 42.9 us -> none  [summed_on_arrival(): blocks = lax.all_to_all(in_blocks(x, dim, peers), axis, 0, 0, tiled=True)]
    psum x2 -> x0, blocking collectives: 39.6 us -> none  [one_axis_at_a_time(): return functools.reduce(lax.psum, axes, x)]
    all_gather x1 -> x0, blocking collectives: 22.7 us -> none  [side_by_side(): out, at, outs = (lax.all_gather(both, axis, axis=dim, tiled=True), 0, [])]
    dot_general x13 -> x0, matrix products: 19.8 us -> none  [the longest x1 3.66 us: shards(): jnp.einsum('nqhgd,chd->nhgqc', query_blocks, context_key_rows, preferred_...]
    all_gather x1 -> x0, waiting for transfers between devices: 14.9 us -> none  [shards(): block_rows = lax.all_gather(hidden_state, 'tp', axis=0, tiled=True)]
    all_to_all x1 -> x0, starting transfers between devices: 7.64 us -> none  [sent_to_all(): lax.all_to_all(jnp.broadcast_to(x[None], (peers, *x.shape)), axis, 0, 0,...]
    reduce_sum x5 -> x0, other arithmetic: 7.2 us -> none  [the longest x1 3.82 us: shards(): jnp.sum(ctx_exp, axis=-1, keepdims=True)]
  transfers between devices with their start and end apart: 4 -> 0, of which waited for: 1 -> 0; matrix products, arithmetic and copies ran while one was open for 11% -> 0% of each run, Pallas kernels for 0% -> 0%
where the time goes in v2:
time: 72.8 us; the launch traced here: 72.7 us
  Pallas kernels  70.9 us (97%)
  local copies, waits for them, and re-layouts  1.77 us (2%)
    pallas_call x1, Pallas kernels, shards(): pl.pallas_call(block_kernel, out_shape=jax.ShapeDtypeStruct((ROWS, WIDTH)...  70.9 us
    unnamed x1, local copies, waits for them, and re-layouts  1.77 us

profile of v2, /device:TPU:1, one launch (start us, length us, event | category | flops | bytes accessed | tf_op | source)
XLA Modules:
  0.0 72.7 jit_solution(12440129027061616936)
XLA Ops:
  0.0 70.9 %block.1 = bf16[96,2048]{1,0:T(8,128)(2,1)} custom-call(bf16[96,2048]{1,0:T(8,128)(2,1)} %lat_hbm.1, bf16[16,2048]{1,0:T(8,128)(2,1)} %ctx_hbm.1, f32[1,2048]{1,0:T(1,128)} %bitcast.4, f32[1,32]{1,0:T(1,128)} %bitcast.5, f32[1,32]{1,0:T(1,128)} %bitcast.6, bf16[32,256]{1,0:T(8,128)(2,1)} %sw_hbm.1, bf16[32,256]{1,0:T(8,128)(2,1)} %cw_hbm.1, ...), custom_call_target="tpu_custom_call" | custom-call | flops 1000000000 | bytes 10000000 | tf_op jit(solution)/shard_map/block/pallas_call | solution.py:415
  70.9 1.8 %copy.16 = bf16[96,2048]{1,0:T(8,128)(2,1)} copy(bf16[96,2048]{1,0:T(8,128)(2,1)} %block.1) | data formatting | bytes 786432

commit v3 on v2

--- a/solution.py
+++ b/solution.py
@@ -62,12 +62,12 @@
     lat_hbm, ctx_hbm, gain_hbm, cond_hbm, cctx_hbm, sw_hbm, cw_hbm, gw_hbm,
     wq_hbm, wk_hbm, wv_hbm, sink_hbm, wo_hbm, freq_hbm,
     out_ref,
-    lat, ctx, gain, cond, cctx, sw, cw, gw, wqkv, sink, wo, freq,
-    rows, parts, ybuf, zsrc, zbuf, gsrc, gbuf, mod, amp, camp,
-    cos_t, sin_t, band, hid, qkv, q, kv, ctxkv,
+    lat, cr, gain, cond, cctx, sw, cw, gw, wqkv, sink, wo, freq,
+    rows, parts, ybuf, zsrc, zbuf, csrc, gsrc, gbuf, mod, amp, camp,
+    cos_t, sin_t, band, hid, chid, qkv, q, kv, ctxkv,
     att, att_mate, wo_mate, opp_src, right_src, left_src, opp_left, opp_right, from_left, from_right,
     l_sem, y_send, y_recv, z_send, z_recv, g_send, g_recv, a_send, a_recv, p_send, p_recv,
-    c_send, c_recv, d_send, d_recv, h_send, h_recv, m_send, m_recv, s_send, s_recv,
+    e_send, e_recv, f_send, f_recv, d_send, d_recv, h_send, h_recv, m_send, m_recv, s_send, s_recv,
 ):
     z, y, x, c = (lax.axis_index(a) for a in ALL)
     tp = x * NC + c
@@ -82,13 +82,14 @@
         return {"y": wrap(y + dy, NY), "x": wrap(x + dx, NX), "c": wrap(c + dc, NC)}
 
     barrier = pltpu.get_barrier_semaphore()
-    peers = [{"z": wrap(z + d, NZ)} for d in range(1, NZ)]
+    peers = [{"z": wrap(z + d, NZ)} for d in (1, -1, 2, -2, 4, -4)]
     peers += [plane_peer(*p) for p in PLANE] + [after, before]
     for peer in peers:
         pl.semaphore_signal(barrier, inc=1, device_id=peer, device_id_type=MESH)
     pairs = [
         (cond_hbm, cond), (cctx_hbm, cctx), (sw_hbm, sw), (cw_hbm, cw), (gw_hbm, gw),
-        (lat_hbm, lat), (freq_hbm, freq), (ctx_hbm, ctx), (gain_hbm, gain), (sink_hbm, sink),
+        (lat_hbm, lat), (freq_hbm, freq), (gain_hbm, gain), (sink_hbm, sink),
+        (ctx_hbm.at[:, pl.ds(0, 1024)], cr.at[0, z]), (ctx_hbm.at[:, pl.ds(1024, 1024)], cr.at[1, z]),
         (wq_hbm, wqkv.at[:, pl.ds(0, 256)]), (wk_hbm, wqkv.at[:, pl.ds(256, 128)]),
         (wv_hbm, wqkv.at[:, pl.ds(384, 128)]), (wo_hbm, wo),
         (lat_hbm, rows.at[rows_at(tp * ROWS, ROWS)]),
@@ -119,47 +120,6 @@
         )
     for copy in local[5:]:
         copy.wait()
-    pl.semaphore_wait(barrier, len(peers))
-
-    sent = []
-
-    def send(src, dst, s_sem, r_sem, k, to):
-        copy = remote(src, dst, s_sem.at[k], r_sem.at[k], to)
-        copy.start()
-        sent.append(copy)
-        return copy
-
-    y_copies = [
-        send(parts.at[wrap(y + d, NY)], ybuf.at[d], y_send, y_recv, d, {"y": wrap(y + d, NY)})
-        for d in range(1, NY)
-    ]
-
-    def piece(chip, core, h):
-        return rows.at[rows_at((chip * NC + core) * ROWS + h * 48, 48)]
-
-    def along(chip, h, k, to):
-        source = lat.at[pl.ds(h * 48, 48)] if chip is None else piece(chip, c, h)
-        slot = piece(x if chip is None else chip, c, h)
-        send(source, slot, a_send, a_recv, k, {"x": to})
-
-    def across_chip(chip, h, k):
-        send(piece(chip, c, h), piece(chip, c, h), p_send, p_recv, k, partner)
-
-    def arrived(chip, h, k):
-        slot = piece(chip, c, h)
-        remote(slot, slot, a_send.at[k], a_recv.at[k], {"x": right}).wait_recv()
-
-    along(None, 0, 0, right)
-    along(None, 1, 1, left)
-    along(None, 1, 2, right)
-    along(None, 0, 3, left)
-    own_slot = rows.at[rows_at(tp * ROWS, ROWS)]
-    send(lat, own_slot, p_send, p_recv, 0, partner)
-    send(wo, wo_mate, m_send, m_recv, 4, partner)
-
-    for copy in y_copies:
-        copy.wait_recv()
-    zsrc[...] = parts[y] + ybuf[1] + ybuf[2] + ybuf[3]
 
     lane = lax.broadcasted_iota(jnp.int32, (64, 128), 1)
     sign = jnp.where(lane % 64 < 32, -1.0, 1.0)
@@ -168,11 +128,6 @@
     row_ids = sp * (GROUP // GRID_W) + lax.broadcasted_iota(jnp.int32, (16, 128), 0)
     row_angle = row_ids.astype(F32) * freq[...]
     row_cos, row_sin = jnp.cos(row_angle), jnp.sin(row_angle) * sign[0:16]
-
-    z_copies = [
-        send(zsrc, zbuf.at[d], z_send, z_recv, d, {"z": wrap(z + d, NZ)})
-        for d in (8, 7, 9, 6, 10, 5, 11, 4, 12, 3, 13, 2, 14, 1, 15)
-    ]
     for i in range(GROUP // GRID_W):
         block = slice(i * GRID_W, i * GRID_W + GRID_W)
         cos_t[block] = jnp.where(lane < 64, jnp.broadcast_to(row_cos[i : i + 1], (64, 128)), col_cos)
@@ -182,6 +137,73 @@
     )
     band[...] = jnp.where((gap >= 0) & (gap <= 2 * WINDOW_REACH), 0.0, MASKED_SCORE)
     kv[1024:, :] = jnp.zeros((64, 256), BF16)
+    pl.semaphore_wait(barrier, len(peers))
+
+    sent = []
+
+    def send(src, dst, s_sem, r_sem, k, to):
+        copy = remote(src, dst, s_sem.at[k], r_sem.at[k], to)
+        copy.start()
+        sent.append(copy)
+        return copy
+
+    y_copies = [
+        send(parts.at[wrap(y + d, NY)], ybuf.at[d], y_send, y_recv, d, {"y": wrap(y + d, NY)})
+        for d in range(1, NY)
+    ]
+
+    def piece(chip, core, h):
+        return rows.at[rows_at((chip * NC + core) * ROWS + h * 48, 48)]
+
+    def along(chip, h, k, to):
+        source = lat.at[pl.ds(h * 48, 48)] if chip is None else piece(chip, c, h)
+        slot = piece(x if chip is None else chip, c, h)
+        send(source, slot, a_send, a_recv, k, {"x": to})
+
+    def across_chip(chip, h, k):
+        send(piece(chip, c, h), piece(chip, c, h), p_send, p_recv, k, partner)
+
+    def arrived(chip, h, k):
+        slot = piece(chip, c, h)
+        remote(slot, slot, a_send.at[k], a_recv.at[k], {"x": right}).wait_recv()
+
+    along(None, 0, 0, right)
+    along(None, 1, 1, left)
+    along(None, 1, 2, right)
+    along(None, 0, 3, left)
+    own_slot = rows.at[rows_at(tp * ROWS, ROWS)]
+    send(lat, own_slot, p_send, p_recv, 0, partner)
+    send(wo, wo_mate, m_send, m_recv, 4, partner)
+
+    side = 1 - 2 * c
+
+    def ctx_send(block, k, to):
+        slot = cr.at[c, block]
+        send(slot, slot, e_send, e_recv, k, {"z": to})
+
+    def ctx_came(block, k):
+        slot = cr.at[c, block]
+        remote(slot, slot, e_send.at[k], e_recv.at[k], partner).wait_recv()
+        send(slot, slot, f_send, f_recv, k, partner)
+
+    def ctx_spread(block, n):
+        ctx_send(block, 3 + n, wrap(z + 1, NZ))
+        ctx_send(block, 7 + n, wrap(z - 1, NZ))
+        ctx_send(block, 11 + n, wrap(z + 2 * side, NZ))
+
+    ctx_send(z, 0, wrap(z + 4, NZ))
+    ctx_send(z, 1, wrap(z - 4, NZ))
+    ctx_spread(z, 0)
+
+    for copy in y_copies:
+        copy.wait_recv()
+    zsrc[...] = parts[y] + ybuf[1] + ybuf[2] + ybuf[3]
+
+    def z_send_to(src, slot, k, d):
+        return send(src, zbuf.at[slot], z_send, z_recv, k, {"z": wrap(z + d, NZ)})
+
+    low = z_send_to(zsrc, 1, 0, 4)
+    high = z_send_to(zsrc, 2, 1, -4)
 
     arrived(left, 0, 0)
     along(left, 0, 4, right)
@@ -190,20 +212,40 @@
     along(right, 1, 5, left)
     across_chip(right, 1, 2)
 
-    for copy in z_copies:
+    low.wait_recv()
+    far_sum = z_send_to(zbuf.at[1], 3, 2, 4)
+    high.wait_recv()
+    ctx_came(wrap(z - 4, NZ), 0)
+    ctx_came(wrap(z + 4, NZ), 1)
+    ctx_send(wrap(z - 4 * side, NZ), 2, wrap(z + 4 * side, NZ))
+    ctx_spread(wrap(z - 4, NZ), 1)
+    ctx_spread(wrap(z + 4, NZ), 2)
+    far_sum.wait_recv()
+    csrc[...] = zsrc[...] + zbuf[1] + zbuf[2] + zbuf[3]
+    near_sums = [z_send_to(csrc, 4, 3, 1), z_send_to(csrc, 5, 4, -1), z_send_to(csrc, 6, 5, -2)]
+    ctx_came(wrap(z + 8, NZ), 2)
+    ctx_spread(wrap(z + 8, NZ), 3)
+    arrived(left, 1, 2)
+    across_chip(left, 1, 3)
+    arrived(right, 0, 3)
+    across_chip(right, 0, 4)
+    for copy in near_sums:
         copy.wait_recv()
-    total = zsrc[...]
-    for d in range(1, NZ):
-        total = total + zbuf[d]
+    total = csrc[...] + zbuf[4] + zbuf[5] + zbuf[6]
     gsrc[...] = total
     gbuf[tp, y] = total
     g_copies = [
         send(gsrc, gbuf.at[tp, y], g_send, g_recv, k, plane_peer(*p)) for k, p in enumerate(PLANE)
     ]
-    arrived(left, 1, 2)
-    across_chip(left, 1, 3)
-    arrived(right, 0, 3)
-    across_chip(right, 0, 4)
+    for n in range(4):
+        step = (0, -4, 4, 8)[n]
+        ctx_came(wrap(z - 1 + step, NZ), 3 + n)
+        ctx_came(wrap(z + 1 + step, NZ), 7 + n)
+        ctx_came(wrap(z - 2 * side + step, NZ), 11 + n)
+    arrived(across, 0, 4)
+    across_chip(across, 0, 5)
+    arrived(across, 1, 5)
+    across_chip(across, 1, 6)
     for copy in g_copies:
         copy.wait_recv()
     for owner in range(NTP):
@@ -214,23 +256,47 @@
     amp[...] = gain[...] * (1.0 + mod[1:2, :])
     camp[...] = gain[...] * (1.0 + mod[5:6, :])
 
-    def normed(value, gains, shifts):
-        floats = value.astype(F32)
-        mean = jnp.mean(floats * floats, axis=-1, keepdims=True)
-        return (floats * lax.rsqrt(mean + NORM_EPS) * gains + shifts).astype(BF16)
-
-    ctx_hidden = normed(ctx[...], camp[...], mod[4:5, :])
-    ctxkv[0, 0] = jnp.dot(ctx_hidden, wqkv[:, 256:512], preferred_element_type=F32).astype(BF16)
-    cz = [
-        send(ctxkv.at[0, 0], ctxkv.at[0, d], c_send, c_recv, d, {"z": wrap(z + d, NZ)})
-        for d in (8, 7, 9, 6, 10, 5, 11, 4, 12, 3, 13, 2, 14, 1, 15)
-    ]
-    cz_of = dict(zip((8, 7, 9, 6, 10, 5, 11, 4, 12, 3, 13, 2, 14, 1, 15), cz))
-
-    arrived(across, 0, 4)
-    across_chip(across, 0, 5)
-    arrived(across, 1, 5)
-    across_chip(across, 1, 6)
+    for k in range(15):
+        slot = cr.at[1 - c, z]
+        remote(slot, slot, f_send.at[k], f_recv.at[k], partner).wait_recv()
+
+    def normed(load, store, gains, shifts):
+        acc = jnp.zeros((16, 128), F32)
+        for j in range(WIDTH // 128):
+            v = load(j).astype(F32)
+            acc = acc + v * v
+        mean = jnp.sum(acc, axis=1, keepdims=True) * (1.0 / WIDTH)
+        inverse = jnp.broadcast_to(lax.rsqrt(mean + NORM_EPS), (16, 128))
+        for j in range(WIDTH // 128):
+            cols = slice(j * 128, j * 128 + 128)
+            v = load(j).astype(F32)
+            store(cols, (v * inverse * gains[:, cols] + shifts[:, cols]).astype(BF16))
+
+    def ctx_step(i, carry):
+        for g in range(4):
+            block = i * 4 + g
+            dst = rows_at(block * CTX_ROWS, CTX_ROWS)
+
+            def load(j):
+                return cr[j // 8, block, :, (j % 8) * 128 : (j % 8) * 128 + 128]
+
+            def store(cols, value):
+                chid[dst, cols] = value
+
+            normed(load, store, camp, mod[4:5, :])
+        return carry
+
+    lax.fori_loop(0, NZ // 4, ctx_step, 0)
+    ctxkv[0] = jnp.dot(chid[...], wqkv[:, 256:512], preferred_element_type=F32).astype(BF16)
+
+    def ctx_half(slot, h):
+        return ctxkv.at[slot, pl.ds(h * 128, 128)]
+
+    send(ctx_half(0, 0), ctx_half(1, 0), d_send, d_recv, 0, {"y": up})
+    send(ctx_half(0, 1), ctx_half(2, 1), d_send, d_recv, 1, {"y": down})
+    send(ctx_half(0, 1), ctx_half(1, 1), d_send, d_recv, 2, {"y": up})
+    send(ctx_half(0, 0), ctx_half(2, 0), d_send, d_recv, 3, {"y": down})
+
     remote(lat, rows.at[rows_at((x * NC + 1 - c) * ROWS, ROWS)], p_send.at[0], p_recv.at[0], partner).wait_recv()
     for chip, h, k in [(left, 0, 1), (right, 1, 2), (left, 1, 3), (right, 0, 4), (across, 0, 5), (across, 1, 6)]:
         slot = piece(chip, 1 - c, h)
@@ -245,16 +311,14 @@
                 for g in range(4):
                     src = rows_at(chip * CHIP + i * 64 + g * 16, 16)
                     dst = rows_at(n * CHIP + i * 64 + g * 16, 16)
-                    acc = jnp.zeros((16, 128), F32)
-                    for j in range(WIDTH // 128):
-                        v = rows[src, j * 128 : j * 128 + 128].astype(F32)
-                        acc = acc + v * v
-                    mean = jnp.sum(acc, axis=1, keepdims=True) * (1.0 / WIDTH)
-                    inverse = jnp.broadcast_to(lax.rsqrt(mean + NORM_EPS), (16, 128))
-                    for j in range(WIDTH // 128):
-                        cols = slice(j * 128, j * 128 + 128)
-                        v = rows[src, cols].astype(F32)
-                        hid[dst, cols] = (v * inverse * amp[:, cols] + mod[0:1, cols]).astype(BF16)
+
+                    def load(j):
+                        return rows[src, j * 128 : j * 128 + 128]
+
+                    def store(cols, value):
+                        hid[dst, cols] = value
+
+                    normed(load, store, amp, mod[0:1, :])
                 return carry
 
             lax.fori_loop(0, CHIP // 64, norm_step, 0)
@@ -284,25 +348,16 @@
         send(kv.at[pl.ds(GROUP, 128)], kv.at[pl.ds(0, 128)], h_send, h_recv, 0, after),
         send(kv.at[pl.ds(128, 128)], kv.at[pl.ds(GROUP + 128, 128)], h_send, h_recv, 1, before),
     ]
-    for d in range(1, 8):
-        cz_of[d].wait_recv()
-    send(ctxkv.at[0, pl.ds(0, 8)], ctxkv.at[1, pl.ds(0, 8)], d_send, d_recv, 0, {"y": up})
-    send(ctxkv.at[0, pl.ds(0, 8)], ctxkv.at[2, pl.ds(0, 8)], d_send, d_recv, 3, {"y": down})
-    for d in range(8, 16):
-        cz_of[d].wait_recv()
-    send(ctxkv.at[0, pl.ds(8, 8)], ctxkv.at[2, pl.ds(8, 8)], d_send, d_recv, 1, {"y": down})
-    send(ctxkv.at[0, pl.ds(8, 8)], ctxkv.at[1, pl.ds(8, 8)], d_send, d_recv, 2, {"y": up})
-
     project((1, 2))
 
     def ctx_arrived(slot, h, k):
-        ref = ctxkv.at[slot, pl.ds(h * 8, 8)]
+        ref = ctx_half(slot, h)
         remote(ref, ref, d_send.at[k], d_recv.at[k], {"y": up}).wait_recv()
 
     ctx_arrived(1, 0, 0)
-    send(ctxkv.at[1, pl.ds(0, 8)], ctxkv.at[3, pl.ds(0, 8)], d_send, d_recv, 4, {"y": up})
+    send(ctx_half(1, 0), ctx_half(3, 0), d_send, d_recv, 4, {"y": up})
     ctx_arrived(2, 1, 1)
-    send(ctxkv.at[2, pl.ds(8, 8)], ctxkv.at[3, pl.ds(8, 8)], d_send, d_recv, 5, {"y": down})
+    send(ctx_half(2, 1), ctx_half(3, 1), d_send, d_recv, 5, {"y": down})
     for copy in halo:
         copy.wait_recv()
     ctx_arrived(1, 1, 2)
@@ -324,8 +379,8 @@
         bias = band[...] + edge
         near = lax.dot_general(both, kv[window, 0:128], nt, preferred_element_type=F32)
         near = near * factor + jnp.concatenate([bias, bias], axis=0)
-        keys = ctxkv[:, :, :, 0:128].reshape(1024, 128)
-        values = ctxkv[:, :, :, 128:256].reshape(1024, 128)
+        keys = ctxkv[:, :, 0:128].reshape(1024, 128)
+        values = ctxkv[:, :, 128:256].reshape(1024, 128)
         far = lax.dot_general(both, keys, nt, preferred_element_type=F32) * factor
         head = lax.broadcasted_iota(jnp.int32, (2 * CHIP, 1), 0)
         sinks = jnp.where(head < CHIP, sink[0:1, 0:1], sink[0:1, 1:2]) * LOG2E
@@ -418,25 +473,25 @@
         in_specs=[pl.BlockSpec(memory_space=pl.ANY)] * 14,
         out_specs=pl.BlockSpec(memory_space=pltpu.VMEM),
         scratch_shapes=[
-            vm((ROWS, WIDTH), BF16), vm((CTX_ROWS, WIDTH), BF16), vm((1, WIDTH), F32),
+            vm((ROWS, WIDTH), BF16), vm((2, NZ, CTX_ROWS, WIDTH // 2), BF16), vm((1, WIDTH), F32),
             vm((1, 32), F32), vm((1, 32), F32),
             vm((32, 256), BF16), vm((32, 256), BF16), vm((32, 256), BF16),
             vm((WIDTH, 512), BF16), vm((1, 2), F32), vm((256, WIDTH), BF16), vm((1, 128), F32),
             vm((GROUP, WIDTH), BF16),
-            vm((4, 4, 128), F32), vm((NY, 4, 128), F32), vm((4, 128), F32), vm((NZ, 4, 128), F32),
-            vm((4, 128), F32), vm((NTP, NY, 4, 128), F32),
+            vm((4, 4, 128), F32), vm((NY, 4, 128), F32), vm((4, 128), F32), vm((7, 4, 128), F32),
+            vm((4, 128), F32), vm((4, 128), F32), vm((NTP, NY, 4, 128), F32),
             vm((8, WIDTH), F32), vm((1, WIDTH), F32), vm((1, WIDTH), F32),
             vm((GROUP, 128), F32), vm((GROUP, 128), F32), vm((CHIP, WIN), F32),
-            vm((2 * CHIP, WIDTH), BF16), vm((2 * CHIP, 512), F32),
+            vm((2 * CHIP, WIDTH), BF16), vm((NZ * CTX_ROWS, WIDTH), BF16), vm((2 * CHIP, 512), F32),
             vm((GROUP, 256), BF16), vm((GROUP + 256 + 64, 256), BF16),
-            vm((NY, NZ, CTX_ROWS, 256), BF16),
+            vm((NY, NZ * CTX_ROWS, 256), BF16),
             vm((NX, NC, ROWS, 256), BF16), vm((NX, ROWS, 256), BF16), vm((256, WIDTH), BF16),
             vm(half, BF16), vm(half, BF16), vm(half, BF16),
             vm(half[1:], BF16), vm(half[1:], BF16), vm(half, BF16), vm(half, BF16),
-            dma((15,)),
-            dma((NY,)), dma((NY,)), dma((NZ,)), dma((NZ,)), dma((31,)), dma((31,)),
+            dma((16,)),
+            dma((NY,)), dma((NY,)), dma((6,)), dma((6,)), dma((31,)), dma((31,)),
             dma((6,)), dma((6,)), dma((7,)), dma((7,)),
-            dma((NZ,)), dma((NZ,)), dma((6,)), dma((6,)), dma((2,)), dma((2,)),
+            dma((15,)), dma((15,)), dma((15,)), dma((15,)), dma((6,)), dma((6,)), dma((2,)), dma((2,)),
             dma((5,)), dma((5,)), dma((6,)), dma((6,)),
         ],
         compiler_params=pltpu.CompilerParams(

time: 72.8 us -> 71.5 us (0.982)
  Pallas kernels: 70.9 us -> 69.5 us
    pallas_call x1, Pallas kernels: 70.9 us -> 69.5 us  [shards(): pl.pallas_call(block_kernel, out_shape=jax.ShapeDtypeStruct((ROWS, WIDTH)...]
where the time goes in v3:
time: 71.5 us; the launch traced here: 71.3 us
  Pallas kernels  69.5 us (97%)
  local copies, waits for them, and re-layouts  1.77 us (2%)
    pallas_call x1, Pallas kernels, shards(): pl.pallas_call(block_kernel, out_shape=jax.ShapeDtypeStruct((ROWS, WIDTH)...  69.5 us
    unnamed x1, local copies, waits for them, and re-layouts  1.77 us

profile of v3, /device:TPU:1, one launch (start us, length us, event | category | flops | bytes accessed | tf_op | source)
XLA Modules:
  0.0 71.3 jit_solution(11214188118444680067)
XLA Ops:
  0.0 69.5 %block.1 = bf16[96,2048]{1,0:T(8,128)(2,1)} custom-call(bf16[96,2048]{1,0:T(8,128)(2,1)} %lat_hbm.1, bf16[16,2048]{1,0:T(8,128)(2,1)} %ctx_hbm.1, f32[1,2048]{1,0:T(1,128)} %bitcast.4, f32[1,32]{1,0:T(1,128)} %bitcast.5, f32[1,32]{1,0:T(1,128)} %bitcast.6, bf16[32,256]{1,0:T(8,128)(2,1)} %sw_hbm.1, bf16[32,256]{1,0:T(8,128)(2,1)} %cw_hbm.1, ...), custom_call_target="tpu_custom_call" | custom-call | flops 1000000000 | bytes 10000000 | tf_op jit(solution)/shard_map/block/pallas_call | solution.py:470
  69.5 1.8 %copy.16 = bf16[96,2048]{1,0:T(8,128)(2,1)} copy(bf16[96,2048]{1,0:T(8,128)(2,1)} %block.1) | data formatting | bytes 786432

commit v4 on v3

--- a/solution.py
+++ b/solution.py
@@ -32,9 +32,9 @@
 BF16 = jnp.bfloat16
 PLANE = [
     (dy, dx, dc)
-    for dy in range(NY)
-    for dx in range(NX)
-    for dc in range(NC)
+    for dy in (2, 1, 3, 0)
+    for dx in (2, 1, 3, 0)
+    for dc in (1, 0)
     if (dy, dx, dc) != (0, 0, 0)
 ]
 
@@ -63,11 +63,11 @@
     wq_hbm, wk_hbm, wv_hbm, sink_hbm, wo_hbm, freq_hbm,
     out_ref,
     lat, cr, gain, cond, cctx, sw, cw, gw, wqkv, sink, wo, freq,
-    rows, parts, ybuf, zsrc, zbuf, csrc, gsrc, gbuf, mod, amp, camp,
+    rows, parts, nbuf, zsrc, zbuf, gsrc, gbuf, mod, amp, camp,
     cos_t, sin_t, band, hid, chid, qkv, q, kv, ctxkv,
     att, att_mate, wo_mate, opp_src, right_src, left_src, opp_left, opp_right, from_left, from_right,
-    l_sem, y_send, y_recv, z_send, z_recv, g_send, g_recv, a_send, a_recv, p_send, p_recv,
-    e_send, e_recv, f_send, f_recv, d_send, d_recv, h_send, h_recv, m_send, m_recv, s_send, s_recv,
+    l_sem, n_send, n_recv, z_send, z_recv, g_send, g_recv, a_send, a_recv, p_send, p_recv,
+    e_send, e_recv, f_send, f_recv, o_send, o_recv, d_send, d_recv, h_send, h_recv, m_send, m_recv, s_send, s_recv,
 ):
     z, y, x, c = (lax.axis_index(a) for a in ALL)
     tp = x * NC + c
@@ -83,13 +83,17 @@
 
     barrier = pltpu.get_barrier_semaphore()
     peers = [{"z": wrap(z + d, NZ)} for d in (1, -1, 2, -2, 4, -4)]
+    peers += [
+        {"z": wrap(z + d, NZ), "y": wrap(y + e, NY)} for d in (1, -1, 2, -2) for e in range(1, NY)
+    ]
     peers += [plane_peer(*p) for p in PLANE] + [after, before]
     for peer in peers:
         pl.semaphore_signal(barrier, inc=1, device_id=peer, device_id_type=MESH)
     pairs = [
         (cond_hbm, cond), (cctx_hbm, cctx), (sw_hbm, sw), (cw_hbm, cw), (gw_hbm, gw),
         (lat_hbm, lat), (freq_hbm, freq), (gain_hbm, gain), (sink_hbm, sink),
-        (ctx_hbm.at[:, pl.ds(0, 1024)], cr.at[0, z]), (ctx_hbm.at[:, pl.ds(1024, 1024)], cr.at[1, z]),
+        (ctx_hbm.at[:, pl.ds(0, 1024)], cr.at[0, 0, z]),
+        (ctx_hbm.at[:, pl.ds(1024, 1024)], cr.at[1, 0, z]),
         (wq_hbm, wqkv.at[:, pl.ds(0, 256)]), (wk_hbm, wqkv.at[:, pl.ds(256, 128)]),
         (wv_hbm, wqkv.at[:, pl.ds(384, 128)]), (wo_hbm, wo),
         (lat_hbm, rows.at[rows_at(tp * ROWS, ROWS)]),
@@ -147,10 +151,13 @@
         sent.append(copy)
         return copy
 
-    y_copies = [
-        send(parts.at[wrap(y + d, NY)], ybuf.at[d], y_send, y_recv, d, {"y": wrap(y + d, NY)})
-        for d in range(1, NY)
-    ]
+    near = [(dz, dy) for dz in (0, 1, -1, 2) for dy in range(NY) if (dz, dy) != (0, 0)]
+    near_copies = []
+    for k, (dz, dy) in enumerate(near):
+        to = wrap(y + dy, NY)
+        near_copies.append(
+            send(parts.at[to], nbuf.at[k], n_send, n_recv, k, {"z": wrap(z + dz, NZ), "y": to})
+        )
 
     def piece(chip, core, h):
         return rows.at[rows_at((chip * NC + core) * ROWS + h * 48, 48)]
@@ -178,13 +185,17 @@
     side = 1 - 2 * c
 
     def ctx_send(block, k, to):
-        slot = cr.at[c, block]
+        slot = cr.at[c, 0, block]
         send(slot, slot, e_send, e_recv, k, {"z": to})
 
+    def ctx_over(block, k):
+        send(cr.at[c, 0, block], cr.at[c, 1, block], o_send, o_recv, k, {"y": wrap(y + 2, NY)})
+
     def ctx_came(block, k):
-        slot = cr.at[c, block]
+        slot = cr.at[c, 0, block]
         remote(slot, slot, e_send.at[k], e_recv.at[k], partner).wait_recv()
         send(slot, slot, f_send, f_recv, k, partner)
+        ctx_over(block, k)
 
     def ctx_spread(block, n):
         ctx_send(block, 3 + n, wrap(z + 1, NZ))
@@ -194,50 +205,51 @@
     ctx_send(z, 0, wrap(z + 4, NZ))
     ctx_send(z, 1, wrap(z - 4, NZ))
     ctx_spread(z, 0)
-
-    for copy in y_copies:
+    ctx_over(z, 15)
+
+    for copy in near_copies:
         copy.wait_recv()
-    zsrc[...] = parts[y] + ybuf[1] + ybuf[2] + ybuf[3]
-
-    def z_send_to(src, slot, k, d):
-        return send(src, zbuf.at[slot], z_send, z_recv, k, {"z": wrap(z + d, NZ)})
-
-    low = z_send_to(zsrc, 1, 0, 4)
-    high = z_send_to(zsrc, 2, 1, -4)
-
+    quad = parts[y]
+    for k in range(len(near)):
+        quad = quad + nbuf[k]
+    zsrc[...] = quad
+
+    def z_send_to(src, slot, d):
+        return send(src, zbuf.at[slot], z_send, z_recv, slot, {"z": wrap(z + d, NZ)})
+
+    low = z_send_to(zsrc, 0, 4)
+    high = z_send_to(zsrc, 1, -4)
+    ctx_came(wrap(z - 1, NZ), 3)
+    ctx_came(wrap(z + 1, NZ), 7)
+    ctx_came(wrap(z - 2 * side, NZ), 11)
+    low.wait_recv()
+    far = z_send_to(zbuf.at[0], 2, 4)
+    high.wait_recv()
+    ctx_came(wrap(z - 4, NZ), 0)
+    ctx_came(wrap(z + 4, NZ), 1)
+    ctx_send(wrap(z - 4 * side, NZ), 2, wrap(z + 4 * side, NZ))
+    ctx_spread(wrap(z - 4, NZ), 1)
+    ctx_spread(wrap(z + 4, NZ), 2)
     arrived(left, 0, 0)
     along(left, 0, 4, right)
     across_chip(left, 0, 1)
     arrived(right, 1, 1)
     along(right, 1, 5, left)
     across_chip(right, 1, 2)
-
-    low.wait_recv()
-    far_sum = z_send_to(zbuf.at[1], 3, 2, 4)
-    high.wait_recv()
-    ctx_came(wrap(z - 4, NZ), 0)
-    ctx_came(wrap(z + 4, NZ), 1)
-    ctx_send(wrap(z - 4 * side, NZ), 2, wrap(z + 4 * side, NZ))
-    ctx_spread(wrap(z - 4, NZ), 1)
-    ctx_spread(wrap(z + 4, NZ), 2)
-    far_sum.wait_recv()
-    csrc[...] = zsrc[...] + zbuf[1] + zbuf[2] + zbuf[3]
-    near_sums = [z_send_to(csrc, 4, 3, 1), z_send_to(csrc, 5, 4, -1), z_send_to(csrc, 6, 5, -2)]
-    ctx_came(wrap(z + 8, NZ), 2)
-    ctx_spread(wrap(z + 8, NZ), 3)
-    arrived(left, 1, 2)
-    across_chip(left, 1, 3)
-    arrived(right, 0, 3)
-    across_chip(right, 0, 4)
-    for copy in near_sums:
-        copy.wait_recv()
-    total = csrc[...] + zbuf[4] + zbuf[5] + zbuf[6]
+    far.wait_recv()
+    total = zsrc[...] + zbuf[0] + zbuf[1] + zbuf[2]
     gsrc[...] = total
     gbuf[tp, y] = total
     g_copies = [
         send(gsrc, gbuf.at[tp, y], g_send, g_recv, k, plane_peer(*p)) for k, p in enumerate(PLANE)
     ]
-    for n in range(4):
+    arrived(left, 1, 2)
+    across_chip(left, 1, 3)
+    arrived(right, 0, 3)
+    across_chip(right, 0, 4)
+    ctx_came(wrap(z + 8, NZ), 2)
+    ctx_spread(wrap(z + 8, NZ), 3)
+    for n in range(1, 4):
         step = (0, -4, 4, 8)[n]
         ctx_came(wrap(z - 1 + step, NZ), 3 + n)
         ctx_came(wrap(z + 1 + step, NZ), 7 + n)
@@ -246,6 +258,10 @@
     across_chip(across, 0, 5)
     arrived(across, 1, 5)
     across_chip(across, 1, 6)
+    for k in range(16):
+        slot = cr.at[c, 1, z]
+        remote(slot, slot, o_send.at[k], o_recv.at[k], partner).wait_recv()
+    send(cr.at[c, 1], cr.at[c, 1], f_send, f_recv, 15, partner)
     for copy in g_copies:
         copy.wait_recv()
     for owner in range(NTP):
@@ -257,7 +273,7 @@
     camp[...] = gain[...] * (1.0 + mod[5:6, :])
 
     for k in range(15):
-        slot = cr.at[1 - c, z]
+        slot = cr.at[1 - c, 0, z]
         remote(slot, slot, f_send.at[k], f_recv.at[k], partner).wait_recv()
 
     def normed(load, store, gains, shifts):
@@ -272,30 +288,31 @@
             v = load(j).astype(F32)
             store(cols, (v * inverse * gains[:, cols] + shifts[:, cols]).astype(BF16))
 
-    def ctx_step(i, carry):
-        for g in range(4):
-            block = i * 4 + g
-            dst = rows_at(block * CTX_ROWS, CTX_ROWS)
-
-            def load(j):
-                return cr[j // 8, block, :, (j % 8) * 128 : (j % 8) * 128 + 128]
-
-            def store(cols, value):
-                chid[dst, cols] = value
-
-            normed(load, store, camp, mod[4:5, :])
-        return carry
-
-    lax.fori_loop(0, NZ // 4, ctx_step, 0)
-    ctxkv[0] = jnp.dot(chid[...], wqkv[:, 256:512], preferred_element_type=F32).astype(BF16)
-
-    def ctx_half(slot, h):
-        return ctxkv.at[slot, pl.ds(h * 128, 128)]
-
-    send(ctx_half(0, 0), ctx_half(1, 0), d_send, d_recv, 0, {"y": up})
-    send(ctx_half(0, 1), ctx_half(2, 1), d_send, d_recv, 1, {"y": down})
-    send(ctx_half(0, 1), ctx_half(1, 1), d_send, d_recv, 2, {"y": up})
-    send(ctx_half(0, 0), ctx_half(2, 0), d_send, d_recv, 3, {"y": down})
+    def ctx_project(column):
+        def ctx_step(i, carry):
+            for g in range(4):
+                block = i * 4 + g
+                dst = rows_at(block * CTX_ROWS, CTX_ROWS)
+
+                def load(j):
+                    return cr[j // 8, column, block, :, (j % 8) * 128 : (j % 8) * 128 + 128]
+
+                def store(cols, value):
+                    chid[dst, cols] = value
+
+                normed(load, store, camp, mod[4:5, :])
+            return carry
+
+        lax.fori_loop(0, NZ // 4, ctx_step, 0)
+        ctxkv[column] = jnp.dot(
+            chid[...], wqkv[:, 256:512], preferred_element_type=F32
+        ).astype(BF16)
+
+    ctx_project(0)
+    ctx_up = send(ctxkv.at[0], ctxkv.at[2], d_send, d_recv, 0, {"y": up})
+    ctx_down = send(ctxkv.at[0], ctxkv.at[3], d_send, d_recv, 1, {"y": down})
+    whole = cr.at[1 - c, 1]
+    remote(whole, whole, f_send.at[15], f_recv.at[15], partner).wait_recv()
 
     remote(lat, rows.at[rows_at((x * NC + 1 - c) * ROWS, ROWS)], p_send.at[0], p_recv.at[0], partner).wait_recv()
     for chip, h, k in [(left, 0, 1), (right, 1, 2), (left, 1, 3), (right, 0, 4), (across, 0, 5), (across, 1, 6)]:
@@ -350,20 +367,11 @@
     ]
     project((1, 2))
 
-    def ctx_arrived(slot, h, k):
-        ref = ctx_half(slot, h)
-        remote(ref, ref, d_send.at[k], d_recv.at[k], {"y": up}).wait_recv()
-
-    ctx_arrived(1, 0, 0)
-    send(ctx_half(1, 0), ctx_half(3, 0), d_send, d_recv, 4, {"y": up})
-    ctx_arrived(2, 1, 1)
-    send(ctx_half(2, 1), ctx_half(3, 1), d_send, d_recv, 5, {"y": down})
+    ctx_project(1)
     for copy in halo:
         copy.wait_recv()
-    ctx_arrived(1, 1, 2)
-    ctx_arrived(2, 0, 3)
-    ctx_arrived(3, 0, 4)
-    ctx_arrived(3, 1, 5)
+    ctx_up.wait_recv()
+    ctx_down.wait_recv()
 
     nt = (((1,), (1,)), ((), ()))
     factor = HEAD_DIM ** (-0.5) * LOG2E
@@ -371,37 +379,42 @@
 
     def attend(chip):
         begin = chip * CHIP
-        at = rows_at(begin, CHIP)
-        both = jnp.concatenate([q[at, 0:128], q[at, 128:256]], axis=0)
         window = rows_at(begin, WIN)
         key_at = last + begin + lax.broadcasted_iota(jnp.int32, (1, WIN), 1)
         edge = jnp.where((key_at >= 0) & (key_at < GROUP * NZ * NY), 0.0, MASKED_SCORE)
-        bias = band[...] + edge
-        near = lax.dot_general(both, kv[window, 0:128], nt, preferred_element_type=F32)
-        near = near * factor + jnp.concatenate([bias, bias], axis=0)
         keys = ctxkv[:, :, 0:128].reshape(1024, 128)
         values = ctxkv[:, :, 128:256].reshape(1024, 128)
-        far = lax.dot_general(both, keys, nt, preferred_element_type=F32) * factor
-        head = lax.broadcasted_iota(jnp.int32, (2 * CHIP, 1), 0)
-        sinks = jnp.where(head < CHIP, sink[0:1, 0:1], sink[0:1, 1:2]) * LOG2E
-        top = jnp.maximum(
-            jnp.maximum(jnp.max(near, axis=1, keepdims=True), jnp.max(far, axis=1, keepdims=True)), sinks
-        )
-        near = jnp.exp2(near - top)
-        far = jnp.exp2(far - top)
-        bottom = (
-            jnp.sum(near, axis=1, keepdims=True)
-            + jnp.sum(far, axis=1, keepdims=True)
-            + jnp.exp2(sinks - top)
-        )
-        mixed = jnp.dot(near.astype(BF16), kv[window, 128:256], preferred_element_type=F32)
-        mixed = mixed + jnp.dot(far.astype(BF16), values, preferred_element_type=F32)
-        mixed = (mixed / bottom).astype(BF16)
-        for h in range(2):
-            for core in range(NC):
-                begin = h * CHIP + core * ROWS
-                att[chip, core, :, h * 128 : h * 128 + 128] = mixed[begin : begin + ROWS]
-        return send(att.at[chip, 1 - c], att_mate.at[chip], m_send, m_recv, chip, partner)
+        head = lax.broadcasted_iota(jnp.int32, (2 * ROWS, 1), 0)
+        sinks = jnp.where(head < ROWS, sink[0:1, 0:1], sink[0:1, 1:2]) * LOG2E
+
+        def part(core):
+            at = rows_at(begin + core * ROWS, ROWS)
+            both = jnp.concatenate([q[at, 0:128], q[at, 128:256]], axis=0)
+            bias = band[rows_at(core * ROWS, ROWS)] + edge
+            near = lax.dot_general(both, kv[window, 0:128], nt, preferred_element_type=F32)
+            near = near * factor + jnp.concatenate([bias, bias], axis=0)
+            far = lax.dot_general(both, keys, nt, preferred_element_type=F32) * factor
+            top = jnp.maximum(
+                jnp.maximum(jnp.max(near, axis=1, keepdims=True), jnp.max(far, axis=1, keepdims=True)),
+                sinks,
+            )
+            near = jnp.exp2(near - top)
+            far = jnp.exp2(far - top)
+            bottom = (
+                jnp.sum(near, axis=1, keepdims=True)
+                + jnp.sum(far, axis=1, keepdims=True)
+                + jnp.exp2(sinks - top)
+            )
+            mixed = jnp.dot(near.astype(BF16), kv[window, 128:256], preferred_element_type=F32)
+            mixed = mixed + jnp.dot(far.astype(BF16), values, preferred_element_type=F32)
+            mixed = (mixed / bottom).astype(BF16)
+            for h in range(2):
+                att[chip, core, :, h * 128 : h * 128 + 128] = mixed[h * ROWS : h * ROWS + ROWS]
+
+        part(1 - c)
+        copy = send(att.at[chip, 1 - c], att_mate.at[chip], m_send, m_recv, chip, partner)
+        part(c)
+        return copy
 
     def product(chip, h):
         cols = slice(h * 1024, h * 1024 + 1024)
@@ -473,13 +486,13 @@
         in_specs=[pl.BlockSpec(memory_space=pl.ANY)] * 14,
         out_specs=pl.BlockSpec(memory_space=pltpu.VMEM),
         scratch_shapes=[
-            vm((ROWS, WIDTH), BF16), vm((2, NZ, CTX_ROWS, WIDTH // 2), BF16), vm((1, WIDTH), F32),
+            vm((ROWS, WIDTH), BF16), vm((2, 2, NZ, CTX_ROWS, WIDTH // 2), BF16), vm((1, WIDTH), F32),
             vm((1, 32), F32), vm((1, 32), F32),
             vm((32, 256), BF16), vm((32, 256), BF16), vm((32, 256), BF16),
             vm((WIDTH, 512), BF16), vm((1, 2), F32), vm((256, WIDTH), BF16), vm((1, 128), F32),
             vm((GROUP, WIDTH), BF16),
-            vm((4, 4, 128), F32), vm((NY, 4, 128), F32), vm((4, 128), F32), vm((7, 4, 128), F32),
-            vm((4, 128), F32), vm((4, 128), F32), vm((NTP, NY, 4, 128), F32),
+            vm((4, 4, 128), F32), vm((15, 4, 128), F32), vm((4, 128), F32), vm((3, 4, 128), F32),
+            vm((4, 128), F32), vm((NTP, NY, 4, 128), F32),
             vm((8, WIDTH), F32), vm((1, WIDTH), F32), vm((1, WIDTH), F32),
             vm((GROUP, 128), F32), vm((GROUP, 128), F32), vm((CHIP, WIN), F32),
             vm((2 * CHIP, WIDTH), BF16), vm((NZ * CTX_ROWS, WIDTH), BF16), vm((2 * CHIP, 512), F32),
@@ -489,9 +502,9 @@
             vm(half, BF16), vm(half, BF16), vm(half, BF16),
             vm(half[1:], BF16), vm(half[1:], BF16), vm(half, BF16), vm(half, BF16),
             dma((16,)),
-            dma((NY,)), dma((NY,)), dma((6,)), dma((6,)), dma((31,)), dma((31,)),
+            dma((15,)), dma((15,)), dma((3,)), dma((3,)), dma((31,)), dma((31,)),
             dma((6,)), dma((6,)), dma((7,)), dma((7,)),
-            dma((15,)), dma((15,)), dma((15,)), dma((15,)), dma((6,)), dma((6,)), dma((2,)), dma((2,)),
+            dma((15,)), dma((15,)), dma((16,)), dma((16,)), dma((16,)), dma((16,)), dma((2,)), dma((2,)), dma((2,)), dma((2,)),
             dma((5,)), dma((5,)), dma((6,)), dma((6,)),
         ],
         compiler_params=pltpu.CompilerParams(

time: 71.5 us -> 72.4 us (1.013)
  Pallas kernels: 69.5 us -> 70.5 us
    pallas_call x1, Pallas kernels: 69.5 us -> 70.5 us  [shards(): pl.pallas_call(block_kernel, out_shape=jax.ShapeDtypeStruct((ROWS, WIDTH)...]
where the time goes in v4:
time: 72.4 us; the launch traced here: 72.3 us
  Pallas kernels  70.5 us (97%)
  local copies, waits for them, and re-layouts  1.77 us (2%)
    pallas_call x1, Pallas kernels, shards(): pl.pallas_call(block_kernel, out_shape=jax.ShapeDtypeStruct((ROWS, WIDTH)...  70.5 us
    unnamed x1, local copies, waits for them, and re-layouts  1.77 us

profile of v4, /device:TPU:1, one launch (start us, length us, event | category | flops | bytes accessed | tf_op | source)
XLA Modules:
  0.0 72.3 jit_solution(16803988685206195117)
XLA Ops:
  0.0 70.5 %block.1 = bf16[96,2048]{1,0:T(8,128)(2,1)} custom-call(bf16[96,2048]{1,0:T(8,128)(2,1)} %lat_hbm.1, bf16[16,2048]{1,0:T(8,128)(2,1)} %ctx_hbm.1, f32[1,2048]{1,0:T(1,128)} %bitcast.4, f32[1,32]{1,0:T(1,128)} %bitcast.5, f32[1,32]{1,0:T(1,128)} %bitcast.6, bf16[32,256]{1,0:T(8,128)(2,1)} %sw_hbm.1, bf16[32,256]{1,0:T(8,128)(2,1)} %cw_hbm.1, ...), custom_call_target="tpu_custom_call" | custom-call | flops 1000000000 | bytes 10000000 | tf_op jit(solution)/shard_map/block/pallas_call | solution.py:483
  70.5 1.8 %copy.16 = bf16[96,2048]{1,0:T(8,128)(2,1)} copy(bf16[96,2048]{1,0:T(8,128)(2,1)} %block.1) | data formatting | bytes 786432

commit v5 on v4

--- a/solution.py
+++ b/solution.py
@@ -258,10 +258,6 @@
     across_chip(across, 0, 5)
     arrived(across, 1, 5)
     across_chip(across, 1, 6)
-    for k in range(16):
-        slot = cr.at[c, 1, z]
-        remote(slot, slot, o_send.at[k], o_recv.at[k], partner).wait_recv()
-    send(cr.at[c, 1], cr.at[c, 1], f_send, f_recv, 15, partner)
     for copy in g_copies:
         copy.wait_recv()
     for owner in range(NTP):
@@ -311,8 +307,6 @@
     ctx_project(0)
     ctx_up = send(ctxkv.at[0], ctxkv.at[2], d_send, d_recv, 0, {"y": up})
     ctx_down = send(ctxkv.at[0], ctxkv.at[3], d_send, d_recv, 1, {"y": down})
-    whole = cr.at[1 - c, 1]
-    remote(whole, whole, f_send.at[15], f_recv.at[15], partner).wait_recv()
 
     remote(lat, rows.at[rows_at((x * NC + 1 - c) * ROWS, ROWS)], p_send.at[0], p_recv.at[0], partner).wait_recv()
     for chip, h, k in [(left, 0, 1), (right, 1, 2), (left, 1, 3), (right, 0, 4), (across, 0, 5), (across, 1, 6)]:
@@ -365,7 +359,13 @@
         send(kv.at[pl.ds(GROUP, 128)], kv.at[pl.ds(0, 128)], h_send, h_recv, 0, after),
         send(kv.at[pl.ds(128, 128)], kv.at[pl.ds(GROUP + 128, 128)], h_send, h_recv, 1, before),
     ]
+    for k in range(16):
+        slot = cr.at[c, 1, z]
+        remote(slot, slot, o_send.at[k], o_recv.at[k], partner).wait_recv()
+    send(cr.at[c, 1], cr.at[c, 1], f_send, f_recv, 15, partner)
     project((1, 2))
+    whole = cr.at[1 - c, 1]
+    remote(whole, whole, f_send.at[15], f_recv.at[15], partner).wait_recv()
 
     ctx_project(1)
     for copy in halo:

time: 72.4 us -> 69 us (0.953)
  Pallas kernels: 70.5 us -> 67.1 us
    pallas_call x1, Pallas kernels: 70.5 us -> 67.1 us  [shards(): pl.pallas_call(block_kernel, out_shape=jax.ShapeDtypeStruct((ROWS, WIDTH)...]
where the time goes in v5:
time: 69 us; the launch traced here: 68.8 us
  Pallas kernels  67.1 us (97%)
  local copies, waits for them, and re-layouts  1.77 us (3%)
    pallas_call x1, Pallas kernels, shards(): pl.pallas_call(block_kernel, out_shape=jax.ShapeDtypeStruct((ROWS, WIDTH)...  67.1 us
    unnamed x1, local copies, waits for them, and re-layouts  1.77 us

profile of v5, /device:TPU:1, one launch (start us, length us, event | category | flops | bytes accessed | tf_op | source)
XLA Modules:
  0.0 68.8 jit_solution(4520912740664353154)
XLA Ops:
  0.0 67.1 %block.1 = bf16[96,2048]{1,0:T(8,128)(2,1)} custom-call(bf16[96,2048]{1,0:T(8,128)(2,1)} %lat_hbm.1, bf16[16,2048]{1,0:T(8,128)(2,1)} %ctx_hbm.1, f32[1,2048]{1,0:T(1,128)} %bitcast.4, f32[1,32]{1,0:T(1,128)} %bitcast.5, f32[1,32]{1,0:T(1,128)} %bitcast.6, bf16[32,256]{1,0:T(8,128)(2,1)} %sw_hbm.1, bf16[32,256]{1,0:T(8,128)(2,1)} %cw_hbm.1, ...), custom_call_target="tpu_custom_call" | custom-call | flops 1000000000 | bytes 10000000 | tf_op jit(solution)/shard_map/block/pallas_call | solution.py:483
  67.1 1.8 %copy.16 = bf16[96,2048]{1,0:T(8,128)(2,1)} copy(bf16[96,2048]{1,0:T(8,128)(2,1)} %block.1) | data formatting | bytes 786432

commit v6 on v5

--- a/solution.py
+++ b/solution.py
@@ -63,7 +63,7 @@
     wq_hbm, wk_hbm, wv_hbm, sink_hbm, wo_hbm, freq_hbm,
     out_ref,
     lat, cr, gain, cond, cctx, sw, cw, gw, wqkv, sink, wo, freq,
-    rows, parts, nbuf, zsrc, zbuf, gsrc, gbuf, mod, amp, camp,
+    rows, parts, nbuf, zsrc, zbuf, gsrc, gbuf, mod, amp, camp, shift, cshift,
     cos_t, sin_t, band, hid, chid, qkv, q, kv, ctxkv,
     att, att_mate, wo_mate, opp_src, right_src, left_src, opp_left, opp_right, from_left, from_right,
     l_sem, n_send, n_recv, z_send, z_recv, g_send, g_recv, a_send, a_recv, p_send, p_recv,
@@ -222,20 +222,31 @@
     ctx_came(wrap(z - 1, NZ), 3)
     ctx_came(wrap(z + 1, NZ), 7)
     ctx_came(wrap(z - 2 * side, NZ), 11)
-    low.wait_recv()
-    far = z_send_to(zbuf.at[0], 2, 4)
-    high.wait_recv()
     ctx_came(wrap(z - 4, NZ), 0)
     ctx_came(wrap(z + 4, NZ), 1)
     ctx_send(wrap(z - 4 * side, NZ), 2, wrap(z + 4 * side, NZ))
     ctx_spread(wrap(z - 4, NZ), 1)
     ctx_spread(wrap(z + 4, NZ), 2)
+    low.wait_recv()
+    far = z_send_to(zbuf.at[0], 2, 4)
+    high.wait_recv()
     arrived(left, 0, 0)
     along(left, 0, 4, right)
     across_chip(left, 0, 1)
     arrived(right, 1, 1)
     along(right, 1, 5, left)
     across_chip(right, 1, 2)
+    ctx_came(wrap(z + 8, NZ), 2)
+    ctx_spread(wrap(z + 8, NZ), 3)
+
+    def ctx_group(n):
+        step = (0, -4, 4, 8)[n]
+        ctx_came(wrap(z - 1 + step, NZ), 3 + n)
+        ctx_came(wrap(z + 1 + step, NZ), 7 + n)
+        ctx_came(wrap(z - 2 * side + step, NZ), 11 + n)
+
+    ctx_group(1)
+    ctx_group(2)
     far.wait_recv()
     total = zsrc[...] + zbuf[0] + zbuf[1] + zbuf[2]
     gsrc[...] = total
@@ -247,13 +258,7 @@
     across_chip(left, 1, 3)
     arrived(right, 0, 3)
     across_chip(right, 0, 4)
-    ctx_came(wrap(z + 8, NZ), 2)
-    ctx_spread(wrap(z + 8, NZ), 3)
-    for n in range(1, 4):
-        step = (0, -4, 4, 8)[n]
-        ctx_came(wrap(z - 1 + step, NZ), 3 + n)
-        ctx_came(wrap(z + 1 + step, NZ), 7 + n)
-        ctx_came(wrap(z - 2 * side + step, NZ), 11 + n)
+    ctx_group(3)
     arrived(across, 0, 4)
     across_chip(across, 0, 5)
     arrived(across, 1, 5)
@@ -265,38 +270,42 @@
             cols = pl.ds((owner * 2 + t) * 128, 128)
             mod[0:4, cols] = gbuf[owner, t]
             mod[4:8, cols] = gbuf[owner, 2 + t]
-    amp[...] = gain[...] * (1.0 + mod[1:2, :])
-    camp[...] = gain[...] * (1.0 + mod[5:6, :])
+    tall = (8, WIDTH)
+    amp[...] = jnp.broadcast_to(gain[...] * (1.0 + mod[1:2, :]), tall)
+    camp[...] = jnp.broadcast_to(gain[...] * (1.0 + mod[5:6, :]), tall)
+    shift[...] = jnp.broadcast_to(mod[0:1, :], tall)
+    cshift[...] = jnp.broadcast_to(mod[4:5, :], tall)
 
     for k in range(15):
         slot = cr.at[1 - c, 0, z]
         remote(slot, slot, f_send.at[k], f_recv.at[k], partner).wait_recv()
 
     def normed(load, store, gains, shifts):
-        acc = jnp.zeros((16, 128), F32)
-        for j in range(WIDTH // 128):
-            v = load(j).astype(F32)
-            acc = acc + v * v
-        mean = jnp.sum(acc, axis=1, keepdims=True) * (1.0 / WIDTH)
-        inverse = jnp.broadcast_to(lax.rsqrt(mean + NORM_EPS), (16, 128))
+        inverses = []
+        for g in range(4):
+            acc = jnp.zeros((16, 128), F32)
+            for j in range(WIDTH // 128):
+                v = load(g, j).astype(F32)
+                acc = acc + v * v
+            mean = jnp.sum(acc, axis=1, keepdims=True) * (1.0 / WIDTH)
+            inverses.append(jnp.broadcast_to(lax.rsqrt(mean + NORM_EPS), (16, 128)))
         for j in range(WIDTH // 128):
             cols = slice(j * 128, j * 128 + 128)
-            v = load(j).astype(F32)
-            store(cols, (v * inverse * gains[:, cols] + shifts[:, cols]).astype(BF16))
+            gain_tile = jnp.concatenate([gains[:, cols]] * 2, axis=0)
+            shift_tile = jnp.concatenate([shifts[:, cols]] * 2, axis=0)
+            for g in range(4):
+                v = load(g, j).astype(F32)
+                store(g, cols, (v * inverses[g] * gain_tile + shift_tile).astype(BF16))
 
     def ctx_project(column):
         def ctx_step(i, carry):
-            for g in range(4):
-                block = i * 4 + g
-                dst = rows_at(block * CTX_ROWS, CTX_ROWS)
-
-                def load(j):
-                    return cr[j // 8, column, block, :, (j % 8) * 128 : (j % 8) * 128 + 128]
-
-                def store(cols, value):
-                    chid[dst, cols] = value
-
-                normed(load, store, camp, mod[4:5, :])
+            def load(g, j):
+                return cr[j // 8, column, i * 4 + g, :, (j % 8) * 128 : (j % 8) * 128 + 128]
+
+            def store(g, cols, value):
+                chid[rows_at((i * 4 + g) * CTX_ROWS, CTX_ROWS), cols] = value
+
+            normed(load, store, camp, cshift)
             return carry
 
         lax.fori_loop(0, NZ // 4, ctx_step, 0)
@@ -316,57 +325,64 @@
     lanes = lax.broadcasted_iota(jnp.int32, (16, 128), 1)
     first = lanes % 64 < 32
 
-    def project(chips):
-        for n, chip in enumerate(chips):
-            def norm_step(i, carry):
-                for g in range(4):
-                    src = rows_at(chip * CHIP + i * 64 + g * 16, 16)
-                    dst = rows_at(n * CHIP + i * 64 + g * 16, 16)
-
-                    def load(j):
-                        return rows[src, j * 128 : j * 128 + 128]
-
-                    def store(cols, value):
-                        hid[dst, cols] = value
-
-                    normed(load, store, amp, mod[0:1, :])
-                return carry
-
-            lax.fori_loop(0, CHIP // 64, norm_step, 0)
-        qkv[...] = jnp.dot(hid[...], wqkv[...], preferred_element_type=F32)
-        for n, chip in enumerate(chips):
-            def turn_step(i, carry):
-                for g in range(2):
-                    at = rows_at(n * CHIP + i * 32 + g * 16, 16)
-                    to = rows_at(chip * CHIP + i * 32 + g * 16, 16)
-                    pad = rows_at(chip * CHIP + i * 32 + g * 16 + WINDOW_REACH, 16)
-                    cosine, sine = cos_t[to], sin_t[to]
-                    for h in range(3):
-                        u = qkv[at, h * 128 : h * 128 + 128]
-                        swapped = jnp.where(first, pltpu.roll(u, 96, 1), pltpu.roll(u, 32, 1))
-                        turned = (u * cosine + swapped * sine).astype(BF16)
-                        if h < 2:
-                            q[to, h * 128 : h * 128 + 128] = turned
-                        else:
-                            kv[pad, 0:128] = turned
-                    kv[pad, 128:256] = qkv[at, 384:512].astype(BF16)
-                return carry
-
-            lax.fori_loop(0, CHIP // 32, turn_step, 0)
-
-    project((0, 3))
     halo = [
-        send(kv.at[pl.ds(GROUP, 128)], kv.at[pl.ds(0, 128)], h_send, h_recv, 0, after),
-        send(kv.at[pl.ds(128, 128)], kv.at[pl.ds(GROUP + 128, 128)], h_send, h_recv, 1, before),
+        remote(kv.at[pl.ds(GROUP, 128)], kv.at[pl.ds(0, 128)], h_send.at[0], h_recv.at[0], after),
+        remote(kv.at[pl.ds(128, 128)], kv.at[pl.ds(GROUP + 128, 128)], h_send.at[1], h_recv.at[1], before),
     ]
+    sent.extend(halo)
     for k in range(16):
         slot = cr.at[c, 1, z]
         remote(slot, slot, o_send.at[k], o_recv.at[k], partner).wait_recv()
     send(cr.at[c, 1], cr.at[c, 1], f_send, f_recv, 15, partner)
-    project((1, 2))
+
+    def project_step(turn, carry):
+        def norm_step(i, carry):
+            chip = turn + (i // 3) * (3 - 2 * turn)
+
+            def load(g, j):
+                src = rows_at(chip * CHIP + (i % 3) * 64 + g * 16, 16)
+                return rows[src, j * 128 : j * 128 + 128]
+
+            def store(g, cols, value):
+                hid[rows_at(i * 64 + g * 16, 16), cols] = value
+
+            normed(load, store, amp, shift)
+            return carry
+
+        lax.fori_loop(0, 2 * CHIP // 64, norm_step, 0)
+        qkv[...] = jnp.dot(hid[...], wqkv[...], preferred_element_type=F32)
+
+        def turn_step(i, carry):
+            chip = turn + (i // 6) * (3 - 2 * turn)
+            for g in range(2):
+                at = rows_at(i * 32 + g * 16, 16)
+                start = chip * CHIP + (i % 6) * 32 + g * 16
+                to = rows_at(start, 16)
+                pad = rows_at(start + WINDOW_REACH, 16)
+                cosine, sine = cos_t[to], sin_t[to]
+                for h in range(3):
+                    u = qkv[at, h * 128 : h * 128 + 128]
+                    swapped = jnp.where(first, pltpu.roll(u, 96, 1), pltpu.roll(u, 32, 1))
+                    turned = (u * cosine + swapped * sine).astype(BF16)
+                    if h < 2:
+                        q[to, h * 128 : h * 128 + 128] = turned
+                    else:
+                        kv[pad, 0:128] = turned
+                kv[pad, 128:256] = qkv[at, 384:512].astype(BF16)
+            return carry
+
+        lax.fori_loop(0, 2 * CHIP // 32, turn_step, 0)
+
+        @pl.when(turn == 0)
+        def _():
+            for copy in halo:
+                copy.start()
+
+        return carry
+
+    lax.fori_loop(0, 2, project_step, 0)
     whole = cr.at[1 - c, 1]
     remote(whole, whole, f_send.at[15], f_recv.at[15], partner).wait_recv()
-
     ctx_project(1)
     for copy in halo:
         copy.wait_recv()
@@ -387,7 +403,11 @@
         head = lax.broadcasted_iota(jnp.int32, (2 * ROWS, 1), 0)
         sinks = jnp.where(head < ROWS, sink[0:1, 0:1], sink[0:1, 1:2]) * LOG2E
 
-        def part(core):
+        copy = remote(att.at[chip, 1 - c], att_mate.at[chip], m_send.at[chip], m_recv.at[chip], partner)
+        sent.append(copy)
+
+        def part(turn, carry):
+            core = lax.rem(1 - c + turn, NC)
             at = rows_at(begin + core * ROWS, ROWS)
             both = jnp.concatenate([q[at, 0:128], q[at, 128:256]], axis=0)
             bias = band[rows_at(core * ROWS, ROWS)] + edge
@@ -411,9 +431,14 @@
             for h in range(2):
                 att[chip, core, :, h * 128 : h * 128 + 128] = mixed[h * ROWS : h * ROWS + ROWS]
 
-        part(1 - c)
-        copy = send(att.at[chip, 1 - c], att_mate.at[chip], m_send, m_recv, chip, partner)
-        part(c)
+
+            @pl.when(turn == 0)
+            def _():
+                copy.start()
+
+            return carry
+
+        lax.fori_loop(0, NC, part, 0)
         return copy
 
     def product(chip, h):
@@ -493,7 +518,7 @@
             vm((GROUP, WIDTH), BF16),
             vm((4, 4, 128), F32), vm((15, 4, 128), F32), vm((4, 128), F32), vm((3, 4, 128), F32),
             vm((4, 128), F32), vm((NTP, NY, 4, 128), F32),
-            vm((8, WIDTH), F32), vm((1, WIDTH), F32), vm((1, WIDTH), F32),
+            vm((8, WIDTH), F32), vm((8, WIDTH), F32), vm((8, WIDTH), F32), vm((8, WIDTH), F32), vm((8, WIDTH), F32),
             vm((GROUP, 128), F32), vm((GROUP, 128), F32), vm((CHIP, WIN), F32),
             vm((2 * CHIP, WIDTH), BF16), vm((NZ * CTX_ROWS, WIDTH), BF16), vm((2 * CHIP, 512), F32),
             vm((GROUP, 256), BF16), vm((GROUP + 256 + 64, 256), BF16),

time: 69 us -> 68.7 us (level)
  no operation moved by 1% of the time
where the time goes in v6:
time: 68.7 us; the launch traced here: 68.6 us
  Pallas kernels  66.8 us (97%)
  local copies, waits for them, and re-layouts  1.77 us (3%)
    pallas_call x1, Pallas kernels, shards(): pl.pallas_call(block_kernel, out_shape=jax.ShapeDtypeStruct((ROWS, WIDTH)...  66.8 us
    unnamed x1, local copies, waits for them, and re-layouts  1.77 us

profile of v6, /device:TPU:1, one launch (start us, length us, event | category | flops | bytes accessed | tf_op | source)
XLA Modules:
  0.0 68.6 jit_solution(5021580579032323685)
XLA Ops:
  0.0 66.8 %block.1 = bf16[96,2048]{1,0:T(8,128)(2,1)} custom-call(bf16[96,2048]{1,0:T(8,128)(2,1)} %lat_hbm.1, bf16[16,2048]{1,0:T(8,128)(2,1)} %ctx_hbm.1, f32[1,2048]{1,0:T(1,128)} %bitcast.4, f32[1,32]{1,0:T(1,128)} %bitcast.5, f32[1,32]{1,0:T(1,128)} %bitcast.6, bf16[32,256]{1,0:T(8,128)(2,1)} %sw_hbm.1, bf16[32,256]{1,0:T(8,128)(2,1)} %cw_hbm.1, ...), custom_call_target="tpu_custom_call" | custom-call | flops 1000000000 | bytes 10000000 | tf_op jit(solution)/shard_map/block/pallas_call | solution.py:508
  66.8 1.8 %copy.16 = bf16[96,2048]{1,0:T(8,128)(2,1)} copy(bf16[96,2048]{1,0:T(8,128)(2,1)} %block.1) | data formatting | bytes 786432
